TPU v7x, 32 devices: a whole 2x2x4 slice. The times are simulated.
32 devices in a mesh: rep: 4 (over z), fs: 4 (over y, x), tp: 2 (over core).
Axes of the slice: x: 2, y: 2, z: 4, core: 2. Of those that a mesh axis runs over, the one named last changes fastest.
Arguments:
- residual: bfloat16 [16, 256, 2048], P(('rep', 'fs'), None, 'tp'), may hold values from -6 to 6
- queries: bfloat16 [16, 256, 2048], P(('rep', 'fs'), None, 'tp'), may hold values from -6 to 6
- key_matrix: bfloat16 [16, 256, 2048], P(('rep', 'fs'), None, 'tp'), may hold values from -6 to 6
- value_matrix: bfloat16 [16, 256, 2048], P(('rep', 'fs'), None, 'tp'), may hold values from -6 to 6
- decay_logodds: float32 [16, 256, 2048], P(('rep', 'fs'), None, 'tp'), may hold values from -3.4 to 8.9, as said below
- decay_surge: float32 [16, 256, 8], P(('rep', 'fs'), None, 'tp'), may hold values from -2.1 to 0, as said below
- head_norm_gain: float32 [256], replicated, may hold values from 0.1 to 1.9
- output_matrix: float32 [2048, 2048], P('fs', 'tp'), may hold values from -0.125 to 0.125
- output_column_scale: float32 [2048], P('tp'), may hold values from 0.5 to 2
- premix_norm_gain: float32 [2048], replicated, may hold values from 0.1 to 1.9
- gate_matrix: float32 [2048, 2816], P('fs', 'tp'), may hold values from -0.125 to 0.125
- gate_column_scale: float32 [2816], P('tp'), may hold values from 0.5 to 2
- up_matrix: float32 [2048, 2816], P('fs', 'tp'), may hold values from -0.125 to 0.125
- up_column_scale: float32 [2816], P('tp'), may hold values from 0.5 to 2
- down_matrix: float32 [2048, 2816], P('fs', 'tp'), may hold values from -0.109375 to 0.109375
- down_column_scale: float32 [2048], P('tp'), may hold values from 0.5 to 2
Outputs:
- layer_out: bfloat16 [16, 256, 2048], P(('rep', 'fs'), None, 'tp')
Inputs may be any that keep to these rules, and one draw needn't show every extreme that they name: `decay_logodds`: log-odds of a key channel's decay. `decay_surge`: non-positive log-factors of a head's state.
All inputs are finite; a program needn't handle non-finite values.
Results may differ from a plain program's by a relative error of at most 0.018.
Values may be sent and summed in bfloat16 or wider, within the bound.
A program may use at most 128 MiB of HBM per device.

v0:
```python
import jax
import jax.numpy as jnp
from jax import lax
from jax.sharding import PartitionSpec as P

BLOCK = 64


epsilon = 1e-06
softness_factor = 16.0
highest = lax.Precision.HIGHEST


def one_direction(query_heads, key_heads, value_heads, log_decay_values):
    sequence_batch, head_total, token_length, key_channel_width = query_heads.shape
    value_width = value_heads.shape[-1]
    block_count = token_length // BLOCK

    def blocks(tensor):
        return tensor.reshape(sequence_batch, head_total, block_count, BLOCK, tensor.shape[-1])

    q_blocks = blocks(query_heads)
    k_blocks = blocks(key_heads)
    v_blocks = blocks(value_heads)
    running = jnp.cumsum(blocks(log_decay_values), axis=3)
    block_end = running[:, :, :, -1:, :]
    q_dec = q_blocks * jnp.exp(running)
    k_inv = k_blocks * jnp.exp(-running)
    k_end = k_blocks * jnp.exp(block_end - running)
    lower_mask = jnp.tril(jnp.ones((BLOCK, BLOCK), jnp.float32))
    scores = jnp.einsum("shnid,shnjd->shnij", q_dec, k_inv, precision=highest) * lower_mask
    inner_part = jnp.einsum("shnij,shnje->shnie", scores, v_blocks, precision=highest)
    fading = jnp.exp(block_end[:, :, :, 0, :])

    def advance(memory, pieces):
        q_piece, k_piece, v_piece, f_piece = pieces
        carried = jnp.einsum("shcd,shde->shce", q_piece, memory, precision=highest)
        memory = f_piece[..., None] * memory + jnp.einsum(
            "shcd,shce->shde", k_piece, v_piece, precision=highest
        )
        return (memory, carried)

    pieces = tuple((jnp.moveaxis(tensor, 2, 0) for tensor in (q_dec, k_end, v_blocks, fading)))
    initial = jnp.zeros((sequence_batch, head_total, key_channel_width, value_width), jnp.float32)
    _, carried = lax.scan(advance, initial, pieces)
    summed = inner_part + jnp.moveaxis(carried, 0, 2)
    return summed.reshape(sequence_batch, head_total, token_length, value_width)


def backwards(tensor):
    return tensor[:, :, ::-1]


def linear_attend(queries, key_matrix, value_matrix, decay_logodds, decay_surge, head_norm_gain):
    sequence_batch, token_length, head_total = decay_surge.shape
    key_channel_width = queries.shape[-1] // head_total
    value_width = value_matrix.shape[-1] // head_total

    def split_heads(tensor, width):
        return jnp.transpose(
            tensor.astype(jnp.float32).reshape(sequence_batch, token_length, head_total, width),
            (0, 2, 1, 3),
        )

    query_heads = split_heads(queries, key_channel_width) * key_channel_width ** (-0.5)
    key_heads = split_heads(key_matrix, key_channel_width)
    value_heads = split_heads(value_matrix, value_width)
    gate_values = (
        jax.nn.log_sigmoid(decay_logodds).reshape(
            sequence_batch, token_length, head_total, key_channel_width
        )
        / softness_factor
    )
    log_decay_values = jnp.transpose(gate_values + decay_surge[..., None], (0, 2, 1, 3))
    forward = one_direction(query_heads, key_heads, value_heads, log_decay_values)
    backward = backwards(
        one_direction(
            backwards(query_heads),
            backwards(key_heads),
            backwards(value_heads),
            backwards(log_decay_values),
        )
    )
    attended = forward + backward
    scaled = (
        attended
        * lax.rsqrt(jnp.mean(attended * attended, axis=-1, keepdims=True) + epsilon)
        * head_norm_gain
    )
    merged = jnp.transpose(scaled, (0, 2, 1, 3)).reshape(
        sequence_batch * token_length, head_total * value_width
    )
    return merged.astype(jnp.bfloat16)


def by_rows(left, right):
    return lax.dot_general(
        left, right, (((1,), (1,)), ((), ())), preferred_element_type=jnp.float32
    )


def body(
    residual,
    queries,
    key_matrix,
    value_matrix,
    decay_logodds,
    decay_surge,
    head_norm_gain,
    output_matrix,
    output_column_scale,
    premix_norm_gain,
    gate_matrix,
    gate_column_scale,
    up_matrix,
    up_column_scale,
    down_matrix,
    down_column_scale,
):
    sequence_batch, token_length, local_width = residual.shape
    row_count = sequence_batch * token_length
    normalized_rows = linear_attend(
        queries, key_matrix, value_matrix, decay_logodds, decay_surge, head_norm_gain
    )
    out_half = output_matrix.astype(jnp.bfloat16)
    out_full = lax.all_gather(out_half, "fs", axis=0, tiled=True)
    mix_terms = by_rows(normalized_rows, out_full)
    mix_total = lax.psum_scatter(
        mix_terms.astype(jnp.bfloat16), "tp", scatter_dimension=1, tiled=True
    ).astype(jnp.float32)
    own_rows = residual.reshape(row_count, local_width).astype(jnp.float32)
    updated = (own_rows + output_column_scale * mix_total).astype(jnp.bfloat16)
    features = lax.all_gather(updated, "tp", axis=1, tiled=True)
    wide_rows = features.astype(jnp.float32)
    factor = lax.rsqrt(jnp.mean(wide_rows * wide_rows, axis=-1, keepdims=True) + epsilon)
    normin = (wide_rows * factor * premix_norm_gain).astype(jnp.bfloat16)
    gate_half = gate_matrix.astype(jnp.bfloat16)
    up_half = up_matrix.astype(jnp.bfloat16)
    down_half = down_matrix.astype(jnp.bfloat16)
    gate_full, up_full, down_full = (
        lax.all_gather(gate_half, "fs", axis=0, tiled=True),
        lax.all_gather(up_half, "fs", axis=0, tiled=True),
        lax.all_gather(down_half, "fs", axis=0, tiled=True),
    )
    gate_pre = jnp.dot(normin, gate_full, preferred_element_type=jnp.float32)
    up_pre = jnp.dot(normin, up_full, preferred_element_type=jnp.float32)
    hidden = (jax.nn.silu(gate_pre * gate_column_scale) * (up_pre * up_column_scale)).astype(
        jnp.bfloat16
    )
    down_terms = by_rows(hidden, down_full)
    down_total = lax.psum_scatter(
        down_terms.astype(jnp.bfloat16), "tp", scatter_dimension=1, tiled=True
    ).astype(jnp.float32)
    result = (updated.astype(jnp.float32) + down_column_scale * down_total).astype(jnp.bfloat16)
    return result.reshape(sequence_batch, token_length, local_width)


def solution(mesh):
    return jax.shard_map(
        body,
        mesh=mesh,
        in_specs=(
            P(("rep", "fs"), None, "tp"),
            P(("rep", "fs"), None, "tp"),
            P(("rep", "fs"), None, "tp"),
            P(("rep", "fs"), None, "tp"),
            P(("rep", "fs"), None, "tp"),
            P(("rep", "fs"), None, "tp"),
            P(),
            P("fs", "tp"),
            P("tp"),
            P(),
            P("fs", "tp"),
            P("tp"),
            P("fs", "tp"),
            P("tp"),
            P("fs", "tp"),
            P("tp"),
        ),
        out_specs=P(("rep", "fs"), None, "tp"),
        check_vma=False,
    )
```

profile of v0, /device:TPU:0, one launch (start us, length us, event | category | flops | bytes accessed | tf_op | source)
XLA Modules:
  0.0 382.0 jit_solution(15835709176157356482)
XLA Ops:
  6.5 2.8 convert_element_type.65
  9.5 0.6 fusion.38
  10.1 0.5 div.26
  10.8 0.3 add_bitcast_fusion
  11.3 1.2 copy.83
  12.5 4.4 %reduce_window_sum.18 = f32[1,4,4,64,256]{4,3,2,1,0:T(8,128)S(1)} reduce-window(f32[1,4,4,64,256]{4,3,2,1,0:T(8,128)} %bitcast.221, f32[]{:T(128)} %constant.50.clone.1), window={size=1x1x1x64x1 pad=0_0x0_0x0_0x63_0x0_0}, to_apply=%region_3.4 | reduce-window | flops 16515072 | bytes 2097156 | tf_op jit(solution)/shard_map/jit(cumsum)/reduce_window_sum | solution.py:25
  17.2 5.2 %rev.17 = f32[1,4,256,256]{3,2,1,0:T(8,128)} reverse(f32[1,4,256,256]{3,2,1,0:T(8,128)S(1)} %bitcast.201), dimensions={2} | reverse | bytes 2097152 | tf_op jit(solution)/shard_map/rev | solution.py:51
  22.5 1.1 transpose.94
  23.6 1.0 copy-done.1
  24.6 1.1 copy.125
  25.7 8.9 %reverse.3 = f32[1,4,256,256]{3,2,1,0:T(8,128)} reverse(f32[1,4,256,256]{3,2,1,0:T(8,128)} %bitcast.223), dimensions={2} | reverse | bytes 2097152 | tf_op jit(solution)/shard_map/reverse
  34.6 2.3 broadcast_multiply_fusion
  36.9 2.0 copy.75
  39.0 8.8 %rev.18 = f32[1,4,256,256]{2,3,1,0:T(8,128)} reverse(bf16[1,4,256,256]{2,3,1,0:T(8,128)(2,1)} %bitcast.214), dimensions={2} | reverse | bytes 1572864 | tf_op jit(solution)/shard_map/rev | solution.py:51
  47.8 2.6 copy.84
  50.4 3.3 multiply_bitcast_fusion
  53.7 1.1 broadcast.94.clone2.1
  54.8 19.1 %while.27 = (s32[]{:T(128)}, f32[1,4,256,256]{3,2,1,0:T(8,128)S(1)}, f32[4,1,4,64,256]{4,3,0,2,1:T(8,128)}, f32[4,1,4,256]{3,1,0,2:T(1,128)S(1)}, f32[4,1,4,64,2...) while((s32[]{:T(128)}, ...), condition=%wide.region_5.6_spmd.clone, body=%wide.region_4.5_spmd.clone.sunk | while | flops 403701760 | bytes 4216940 | solution.py:45
  54.8 2.5 fusion.87
  57.3 2.3 fusion.86
  59.6 2.5 fusion.87
  62.0 2.3 fusion.86
  64.3 2.5 fusion.87
  66.8 2.3 fusion.86
  69.1 2.5 fusion.87
  71.6 2.3 fusion.86
  73.9 2.5 copy.73
  76.4 1.3 copy.77
  77.7 2.1 copy.76
  79.8 3.0 convolution_multiply_fusion.2
  82.8 1.1 fusion.36
  83.9 1.4 copy.91
  85.3 9.4 %rev.19 = f32[1,4,256,256]{2,3,1,0:T(8,128)} reverse(f32[1,4,256,256]{2,3,1,0:T(8,128)} %copy.91), dimensions={2} | reverse | bytes 2097152 | tf_op jit(solution)/shard_map/rev | solution.py:51
  94.7 4.4 %reduce_window_sum.17 = f32[1,4,4,64,256]{4,3,2,1,0:T(8,128)S(1)} reduce-window(f32[1,4,4,64,256]{4,3,2,1,0:T(8,128)} %bitcast.220, f32[]{:T(128)} %constant.50.clone.1), window={size=1x1x1x64x1 pad=0_0x0_0x0_0x63_0x0_0}, to_apply=%region_0.1 | reduce-window | flops 16515072 | bytes 2097156 | tf_op jit(solution)/shard_map/jit(cumsum)/reduce_window_sum | solution.py:25
  99.1 1.3 broadcast_multiply_fusion.1
  100.4 2.2 convolution_multiply_fusion.3
  102.6 1.7 multiply_bitcast_fusion.2
  104.4 16.6 %while.26 = (s32[]{:T(128)}, f32[1,4,256,256]{3,2,1,0:T(8,128)S(1)}, f32[4,1,4,64,256]{4,3,0,2,1:T(8,128)S(1)}, f32[4,1,4,256]{3,1,0,2:T(1,128)S(1)}, f32[4,1,4,...) while((s32[]{:T(128)}, ...), condition=%wide.region_2.3_spmd.clone, body=%wide.region_1.2_spmd.clone.sunk | while | flops 403701760 | bytes 4216940 | solution.py:45
  104.6 1.8 fusion.81
  106.4 2.3 fusion.80
  108.7 1.7 fusion.81
  110.5 2.3 fusion.80
  112.8 1.8 fusion.81
  114.5 2.3 fusion.80
  116.9 1.7 fusion.81
  118.6 2.3 fusion.80
  121.0 1.8 fusion.35
  122.8 0.3 copy.92
  123.3 0.5 copy-done.16
  124.0 4.6 %convolution_convert_fusion = bf16[256,2048]{1,0:T(8,128)(2,1)} fusion(bf16[256,1024]{0,1:T(8,128)(2,1)S(1)} %bitcast.225, bf16[2048,1024]{1,0:T(8,128)(2,1)} %all-gather.6.cloned.1.call-done), kind=kOutput, calls=%fused_computation.44 | convolution fusion | flops 1074266112 | bytes 5767168 | tf_op jit(solution)/shard_map/dot_general | solution.py:97
  128.6 11.2 %reduce-scatter.3.cloned.1.call-done = bf16[256,1024]{1,0:T(8,128)(2,1)} async-done(((bf16[256,2048]{1,0:T(8,128)(2,1)}), bf16[256,1024]{1,0:T(8,128)(2,1)}) %reduce-scatter.3.cloned.1.call-update) | async-done | bytes 524304 | tf_op jit(solution)/shard_map/reduce_scatter | solution.py:128
  139.9 2.0 fusion.39
  142.0 1.3 convert_element_type.72
  143.4 3.2 convert_element_type.73
  146.7 1.2 convert_element_type.75
  148.0 4.3 %all-gather.8.cloned.1.call-done = bf16[256,2048]{1,0:T(8,128)(2,1)} async-done(((bf16[256,1024]{1,0:T(8,128)(2,1)}), bf16[256,2048]{1,0:T(8,128)(2,1)}) %all-gather.8.cloned.1.call-update) | async-done | bytes 1048592 | tf_op jit(solution)/shard_map/all_gather | solution.py:133
  152.3 1.5 fusion.32
  153.8 67.0 %all-gather.10.cloned.1.call-done = bf16[2048,1408]{1,0:T(8,128)(2,1)} async-done(((bf16[512,1408]{1,0:T(8,128)(2,1)}), bf16[2048,1408]{1,0:T(8,128)(2,1)}) %all-gather.10.cloned.1.call-update) | async-done | bytes 5767184 | tf_op jit(solution)/shard_map/all_gather | solution.py:141
  220.8 4.8 %convolution_multiply_fusion.1 = f32[256,1408]{1,0:T(8,128)S(1)} fusion(bf16[2048,1408]{1,0:T(8,128)(2,1)} %all-gather.10.cloned.1.call-done, f32[1408]{0:T(1024)S(1)} %copy-done.17, bf16[256,2048]{1,0:T(8,128)(2,1)} %all-gather.8.cloned.1.call-done, f32[2048]{0:T(1024)S(1)} %copy-done.18, f32[256]{0:T(256)S(1)} %add_rsqrt_fusion.1), kind=kOutput, calls=%fused_computation.41 | convolution fusion | flops 1478852608 | bytes 8272384 | tf_op jit(solution)/shard_map/dot_general | solution.py:145
  225.7 62.5 %all-gather.12.cloned.1.call-done = bf16[2048,1408]{1,0:T(8,128)(2,1)} async-done(((bf16[512,1408]{1,0:T(8,128)(2,1)}), bf16[2048,1408]{1,0:T(8,128)(2,1)}) %all-gather.12.cloned.1.call-update) | async-done | bytes 5767184 | tf_op jit(solution)/shard_map/all_gather | solution.py:142
  288.2 67.4 %all-gather.14.cloned.1.call-done = bf16[2048,1408]{1,0:T(8,128)(2,1)} async-done(((bf16[512,1408]{1,0:T(8,128)(2,1)}), bf16[2048,1408]{1,0:T(8,128)(2,1)}) %all-gather.14.cloned.1.call-update) | async-done | bytes 5767184 | tf_op jit(solution)/shard_map/all_gather | solution.py:143
  355.6 8.9 %convolution_convert_fusion.1 = bf16[256,2048]{1,0:T(8,128)(2,1)} fusion(bf16[2048,1408]{1,0:T(8,128)(2,1)} %all-gather.14.cloned.1.call-done, bf16[2048,1408]{1,0:T(8,128)(2,1)} %all-gather.12.cloned.1.call-done, f32[256,1408]{1,0:T(8,128)S(1)} %convolution_multiply_fusion.1, f32[1408]{0:T(1024)S(1)} %copy-done.19, bf16[256,2048]{1,0:T(8,128)(2,1)S(1)} %copy-done.9, ...), kind=kOutput, calls=%fused_computation.46 | convolution fusion | flops 2957934592 | bytes 15088128 | tf_op jit(solution)/shard_map/dot_general | solution.py:97
  364.6 8.6 %reduce-scatter.5.cloned.1.call-done = bf16[256,1024]{1,0:T(8,128)(2,1)} async-done(((bf16[256,2048]{1,0:T(8,128)(2,1)}), bf16[256,1024]{1,0:T(8,128)(2,1)}) %reduce-scatter.5.cloned.1.call-update) | async-done | bytes 524304 | tf_op jit(solution)/shard_map/reduce_scatter | solution.py:151
  373.2 2.0 fusion.46
  (85 shorter events, 1.5 us)
Async XLA Ops:
  6.5 2.9 copy-start.10
  6.5 117.4 %all-gather.6.cloned.1.call-start = ((), (), s32[]{:S(2)}) async-start(), calls=%async_computation.2 | async-start | bytes 5242880 | tf_op jit(solution)/shard_map/all_gather | solution.py:126
  9.4 130.4 %reduce-scatter.3.cloned.1.call-start = ((), (), s32[]{:S(2)}) async-start(), calls=%async_computation.3 | async-start | bytes 1572864 | tf_op jit(solution)/shard_map/reduce_scatter | solution.py:128
  9.5 1.1 copy-start.15
  11.1 1.4 copy-start.2
  12.5 4.5 %copy-start.11 = (bf16[1,256,1024]{2,1,0:T(8,128)(2,1)S(1)}, bf16[1,256,1024]{2,1,0:T(8,128)(2,1)}, u32[]{:S(2)}) copy-start(bf16[1,256,1024]{2,1,0:T(8,128)(2,1)} %param.22) | copy-start | bytes 1572868
  23.6 1.0 copy-start.1
  73.9 2.5 copy-start.3
  79.8 3.0 copy-start
  79.8 3.1 copy-start.5
  120.9 2.2 copy-start.6
  123.1 0.7 copy-start.16
  124.0 15.9 %copy-start.12 = (bf16[1,256,1024]{2,1,0:T(8,128)(2,1)S(1)}, bf16[1,256,1024]{2,1,0:T(8,128)(2,1)}, u32[]{:S(2)}) copy-start(bf16[1,256,1024]{2,1,0:T(8,128)(2,1)} %param.20) | copy-start | bytes 1572868
  124.0 15.9 %copy-start.13 = (f32[1024]{0:T(1024)S(1)}, f32[1024]{0:T(1024)}, u32[]{:S(2)}) copy-start(f32[1024]{0:T(1024)} %param.28) | copy-start | bytes 12292
  128.6 13.4 %copy-start.7 = (f32[512,1408]{1,0:T(8,128)S(1)}, f32[512,1408]{1,0:T(8,128)}, u32[]{:S(2)}) copy-start(f32[512,1408]{1,0:T(8,128)} %param.30) | copy-start | bytes 8650756
  128.6 23.7 %all-gather.8.cloned.1.call-start = ((), (), s32[]{:S(2)}) async-start(), calls=%async_computation.4 | async-start | bytes 1572864 | tf_op jit(solution)/shard_map/all_gather | solution.py:133
  141.9 78.9 %all-gather.10.cloned.1.call-start = ((), (), s32[]{:S(2)}) async-start(), calls=%async_computation.5 | async-start | bytes 7208960 | tf_op jit(solution)/shard_map/all_gather | solution.py:141
  143.3 3.4 copy-start.8
  143.3 144.9 %all-gather.12.cloned.1.call-start = ((), (), s32[]{:S(2)}) async-start(), calls=%async_computation.6 | async-start | bytes 7208960 | tf_op jit(solution)/shard_map/all_gather | solution.py:142
  146.6 209.0 %all-gather.14.cloned.1.call-start = ((), (), s32[]{:S(2)}) async-start(), calls=%async_computation.7 | async-start | bytes 7208960 | tf_op jit(solution)/shard_map/all_gather | solution.py:143
  147.9 72.9 %copy-start.17 = (f32[1408]{0:T(1024)S(1)}, f32[1408]{0:T(1024)}, u32[]{:S(2)}) copy-start(f32[1408]{0:T(1024)} %param.31) | copy-start | bytes 16900
  147.9 72.9 %copy-start.18 = (f32[2048]{0:T(1024)S(1)}, f32[2048]{0:T(1024)}, u32[]{:S(2)}) copy-start(f32[2048]{0:T(1024)} %param.29) | copy-start | bytes 24580
  147.9 225.2 %reduce-scatter.5.cloned.1.call-start = ((), (), s32[]{:S(2)}) async-start(), calls=%async_computation.8 | async-start | bytes 1572864 | tf_op jit(solution)/shard_map/reduce_scatter | solution.py:151
  153.8 201.8 %copy-start.9 = (bf16[256,2048]{1,0:T(8,128)(2,1)S(1)}, bf16[256,2048]{1,0:T(8,128)(2,1)}, u32[]{:S(2)}) copy-start(bf16[256,2048]{1,0:T(8,128)(2,1)} %all-gather.8.cloned.1.call-done) | copy-start | bytes 3145732
  153.8 201.8 %copy-start.19 = (f32[1408]{0:T(1024)S(1)}, f32[1408]{0:T(1024)}, u32[]{:S(2)}) copy-start(f32[1408]{0:T(1024)} %param.33) | copy-start | bytes 16900
  225.7 147.5 %copy-start.4 = (bf16[256,1024]{1,0:T(8,128)(2,1)S(1)}, bf16[256,1024]{1,0:T(8,128)(2,1)}, u32[]{:S(2)}) copy-start(bf16[256,1024]{1,0:T(8,128)(2,1)} %fusion.39) | copy-start | bytes 1572868
  225.7 147.5 %copy-start.14 = (f32[1024]{0:T(1024)S(1)}, f32[1024]{0:T(1024)}, u32[]{:S(2)}) copy-start(f32[1024]{0:T(1024)} %param.35) | copy-start | bytes 12292
Sparse Core Ops, SparseCore 0:
  9.5 55.2 all-gather.5
  128.7 11.1 reduce-scatter.2
  142.0 10.1 all-gather.7
  154.0 66.8 all-gather.9
  222.5 65.6 all-gather.11
  289.9 65.6 all-gather.13
  364.7 8.3 reduce-scatter.4
where the time goes:
time: 385 us; the launch traced here: 382 us
  waiting for transfers between devices  221 us (57%)
  matrix products  61.5 us (16%)
  local copies, waits for them, and re-layouts  50.7 us (13%)
  other arithmetic  34.1 us (9%)
  between operations  13.9 us (4%)
    all_gather x1, waiting for transfers between devices, body(): lax.all_gather(down_half, 'fs', axis=0, tiled=True)  67.4 us
    all_gather x1, waiting for transfers between devices, body(): lax.all_gather(gate_half, 'fs', axis=0, tiled=True)  67 us
    all_gather x1, waiting for transfers between devices, body(): lax.all_gather(up_half, 'fs', axis=0, tiled=True)  62.5 us
    rev x6, local copies, waits for them, and re-layouts, backwards(): return tensor[:, :, ::-1]  27.4 us
    dot_general x8, matrix products, advance(): jnp.einsum('shcd,shce->shde', k_piece, v_piece, precision=highest)  18.3 us
    dot_general x8, matrix products, advance(): carried = jnp.einsum('shcd,shde->shce', q_piece, memory, precision=highest)  16.9 us
    dot_general x2, matrix products, by_rows(): lax.dot_general(left, right, (((1,), (1,)), ((), ())), preferred_element_...  13.5 us
    reduce_scatter x1, waiting for transfers between devices, body(): lax.psum_scatter(mix_terms.astype(jnp.bfloat16), 'tp', scatter_dimension=...  11.2 us
  transfers between devices with their start and end apart: 7, of which 6 were waited for; matrix products, arithmetic and copies ran while one was open for 33% of the time, Pallas kernels for 0%

commit v1 on v0

v1 whole, which is shorter than its diff:
```python
import functools

import jax
import jax.numpy as jnp
from jax import lax
from jax.experimental import pallas as pl
from jax.experimental.pallas import tpu as pltpu
from jax.sharding import PartitionSpec as P

BLOCK = 64


epsilon = 1e-06
softness_factor = 16.0
highest = lax.Precision.HIGHEST


def attend_head(q, k, v, logodds, surge, gain):
    tokens, width = q.shape
    blocks = tokens // BLOCK
    mid = BLOCK // 2 - 1
    decay = (
        jnp.minimum(logodds, 0.0) - jnp.log1p(jnp.exp(-jnp.abs(logodds)))
    ) * (1.0 / softness_factor) + surge
    row = lax.broadcasted_iota(jnp.int32, (BLOCK, BLOCK), 0)
    col = lax.broadcasted_iota(jnp.int32, (BLOCK, BLOCK), 1)
    tri = jnp.where(row >= col, 1.0, 0.0).astype(jnp.bfloat16)
    q = q.astype(jnp.float32) * width ** (-0.5)
    k = k.astype(jnp.float32)
    high = decay.astype(jnp.bfloat16)
    low = (decay - high.astype(jnp.float32)).astype(jnp.bfloat16)
    pieces = []
    for n in range(blocks):
        rows = slice(n * BLOCK, (n + 1) * BLOCK)
        running = jnp.dot(tri, high[rows], preferred_element_type=jnp.float32) + jnp.dot(
            tri, low[rows], preferred_element_type=jnp.float32
        )
        before = running - decay[rows]
        center = running[mid : mid + 1]
        end = running[BLOCK - 1 : BLOCK]
        to_center = jnp.exp(center)
        from_center = jnp.exp(end - center)
        q_forward = q[rows] * jnp.exp(running - center)
        k_forward = k[rows] * jnp.exp(center - running)
        q_backward = q[rows] * jnp.exp(center - before)
        k_backward = k[rows] * jnp.exp(before - center)
        half = jnp.bfloat16
        scores = jnp.where(
            row >= col, by_rows(q_forward.astype(half), k_forward.astype(half)), 0.0
        ) + jnp.where(row <= col, by_rows(q_backward.astype(half), k_backward.astype(half)), 0.0)
        inner = jnp.dot(scores.astype(half), v[rows], preferred_element_type=jnp.float32)
        pieces.append(
            (
                inner,
                (q_forward * to_center).astype(half),
                (q_backward * from_center).astype(half),
                by_columns(v[rows], (k_forward * from_center).astype(half)),
                by_columns(v[rows], (k_backward * to_center).astype(half)),
                jnp.exp(end),
            )
        )
    totals = [piece[0] for piece in pieces]
    state = None
    for n in range(blocks):
        if state is not None:
            totals[n] = totals[n] + by_rows(pieces[n][1], state.astype(jnp.bfloat16))
        state = pieces[n][3] if state is None else pieces[n][5] * state + pieces[n][3]
    state = None
    for n in reversed(range(blocks)):
        if state is not None:
            totals[n] = totals[n] + by_rows(pieces[n][2], state.astype(jnp.bfloat16))
        state = pieces[n][4] if state is None else pieces[n][5] * state + pieces[n][4]
    attended = jnp.concatenate(totals, axis=0)
    scale = lax.rsqrt(jnp.mean(attended * attended, axis=-1, keepdims=True) + epsilon)
    return (attended * scale * gain).astype(jnp.bfloat16)


def by_columns(left, right):
    return lax.dot_general(
        left, right, (((0,), (0,)), ((), ())), preferred_element_type=jnp.float32
    )


def attend_kernel(head_total, q_ref, k_ref, v_ref, lo_ref, sg_ref, gain_ref, out_ref):
    width = q_ref.shape[1] // head_total
    value_width = v_ref.shape[1] // head_total
    for h in range(head_total):
        keys = slice(h * width, (h + 1) * width)
        values = slice(h * value_width, (h + 1) * value_width)
        out_ref[:, values] = attend_head(
            q_ref[:, keys],
            k_ref[:, keys],
            v_ref[:, values],
            lo_ref[:, keys],
            sg_ref[:, h : h + 1],
            gain_ref[...],
        )


def linear_attend(queries, key_matrix, value_matrix, decay_logodds, decay_surge, head_norm_gain):
    _, token_length, head_total = decay_surge.shape
    outs = [
        pl.pallas_call(
            functools.partial(attend_kernel, head_total),
            out_shape=jax.ShapeDtypeStruct(value_matrix.shape[1:], jnp.bfloat16),
            in_specs=[pl.BlockSpec(memory_space=pltpu.VMEM)] * 6,
            out_specs=pl.BlockSpec(memory_space=pltpu.VMEM),
            cost_estimate=pl.CostEstimate(
                flops=10**9, bytes_accessed=4 * 10**6, transcendentals=10**6
            ),
        )(
            queries[b], key_matrix[b], value_matrix[b], decay_logodds[b], decay_surge[b],
            head_norm_gain.reshape(1, -1),
        )
        for b in range(queries.shape[0])
    ]
    return jnp.concatenate(outs, axis=0)


def by_rows(left, right):
    return lax.dot_general(
        left, right, (((1,), (1,)), ((), ())), preferred_element_type=jnp.float32
    )


def body(
    residual,
    queries,
    key_matrix,
    value_matrix,
    decay_logodds,
    decay_surge,
    head_norm_gain,
    output_matrix,
    output_column_scale,
    premix_norm_gain,
    gate_matrix,
    gate_column_scale,
    up_matrix,
    up_column_scale,
    down_matrix,
    down_column_scale,
):
    sequence_batch, token_length, local_width = residual.shape
    row_count = sequence_batch * token_length
    normalized_rows = linear_attend(
        queries, key_matrix, value_matrix, decay_logodds, decay_surge, head_norm_gain
    )
    out_half = output_matrix.astype(jnp.bfloat16)
    out_full = lax.all_gather(out_half, "fs", axis=0, tiled=True)
    mix_terms = by_rows(normalized_rows, out_full)
    mix_total = lax.psum_scatter(
        mix_terms.astype(jnp.bfloat16), "tp", scatter_dimension=1, tiled=True
    ).astype(jnp.float32)
    own_rows = residual.reshape(row_count, local_width).astype(jnp.float32)
    updated = (own_rows + output_column_scale * mix_total).astype(jnp.bfloat16)
    features = lax.all_gather(updated, "tp", axis=1, tiled=True)
    wide_rows = features.astype(jnp.float32)
    factor = lax.rsqrt(jnp.mean(wide_rows * wide_rows, axis=-1, keepdims=True) + epsilon)
    normin = (wide_rows * factor * premix_norm_gain).astype(jnp.bfloat16)
    gate_half = gate_matrix.astype(jnp.bfloat16)
    up_half = up_matrix.astype(jnp.bfloat16)
    down_half = down_matrix.astype(jnp.bfloat16)
    gate_full, up_full, down_full = (
        lax.all_gather(gate_half, "fs", axis=0, tiled=True),
        lax.all_gather(up_half, "fs", axis=0, tiled=True),
        lax.all_gather(down_half, "fs", axis=0, tiled=True),
    )
    gate_pre = jnp.dot(normin, gate_full, preferred_element_type=jnp.float32)
    up_pre = jnp.dot(normin, up_full, preferred_element_type=jnp.float32)
    hidden = (jax.nn.silu(gate_pre * gate_column_scale) * (up_pre * up_column_scale)).astype(
        jnp.bfloat16
    )
    down_terms = by_rows(hidden, down_full)
    down_total = lax.psum_scatter(
        down_terms.astype(jnp.bfloat16), "tp", scatter_dimension=1, tiled=True
    ).astype(jnp.float32)
    result = (updated.astype(jnp.float32) + down_column_scale * down_total).astype(jnp.bfloat16)
    return result.reshape(sequence_batch, token_length, local_width)


def solution(mesh):
    return jax.shard_map(
        body,
        mesh=mesh,
        in_specs=(
            P(("rep", "fs"), None, "tp"),
            P(("rep", "fs"), None, "tp"),
            P(("rep", "fs"), None, "tp"),
            P(("rep", "fs"), None, "tp"),
            P(("rep", "fs"), None, "tp"),
            P(("rep", "fs"), None, "tp"),
            P(),
            P("fs", "tp"),
            P("tp"),
            P(),
            P("fs", "tp"),
            P("tp"),
            P("fs", "tp"),
            P("tp"),
            P("fs", "tp"),
            P("tp"),
        ),
        out_specs=P(("rep", "fs"), None, "tp"),
        check_vma=False,
    )
```

time: 385 us -> 320 us (0.83)
  local copies, waits for them, and re-layouts: 50.7 us -> 0.85 us
  waiting for transfers between devices: 221 us -> 265 us
  matrix products: 61.5 us -> 18.4 us
  other arithmetic: 34.1 us -> 14.1 us
  Pallas kernels: 0 us -> 8.08 us
    all_gather x1, waiting for transfers between devices: 0.02 us -> 46.5 us  [body(): out_full = lax.all_gather(out_half, 'fs', axis=0, tiled=True)]
    dot_general x20 -> x0, matrix products: 43.2 us -> none  [the longest x8 18.3 us: advance(): jnp.einsum('shcd,shce->shde', k_piece, v_piece, precision=highest)]
    rev x6 -> x0, local copies, waits for them, and re-layouts: 27.4 us -> none  [backwards(): return tensor[:, :, ::-1]]
    another operation x3 -> x0, local copies, waits for them, and re-layouts: 10.1 us -> none
    another operation x2 -> x0, other arithmetic: 8.77 us -> none  [one_direction(): running = jnp.cumsum(blocks(log_decay_values), axis=3)]
    pallas_call x0 -> x1, Pallas kernels: none -> 8.08 us  [linear_attend(): pl.pallas_call(functools.partial(attend_kernel, head_total), out_shape=ja...]
    transpose x5 -> x0, local copies, waits for them, and re-layouts: 7.07 us -> none  [the longest x4 4.59 us: split_heads(): jnp.transpose(tensor.astype(jnp.float32).reshape(sequence_batch, token_le...]
    transpose x5 -> x0, other arithmetic: 6.57 us -> none  [the longest x2 4.98 us: one_direction(): jnp.moveaxis(tensor, 2, 0)]
  transfers between devices with their start and end apart: 7 -> 7, of which waited for: 6 -> 7; matrix products, arithmetic and copies ran while one was open for 33% -> 4% of each run, Pallas kernels for 0% -> 3%
where the time goes in v1:
time: 320 us
  waiting for transfers between devices  265 us (83%)
  matrix products  18.4 us (6%)
  other arithmetic  14.1 us (4%)
  between operations  13.6 us (4%)
  Pallas kernels  8.08 us (3%)
    all_gather x1, waiting for transfers between devices, body(): lax.all_gather(down_half, 'fs', axis=0, tiled=True)  67.4 us
    all_gather x1, waiting for transfers between devices, body(): lax.all_gather(gate_half, 'fs', axis=0, tiled=True)  67 us
    all_gather x1, waiting for transfers between devices, body(): lax.all_gather(up_half, 'fs', axis=0, tiled=True)  62.5 us
    all_gather x1, waiting for transfers between devices, body(): out_full = lax.all_gather(out_half, 'fs', axis=0, tiled=True)  46.5 us
    dot_general x2, matrix products, by_rows(): lax.dot_general(left, right, (((1,), (1,)), ((), ())), preferred_element_...  13.6 us
    reduce_scatter x1, waiting for transfers between devices, body(): lax.psum_scatter(down_terms.astype(jnp.bfloat16), 'tp', scatter_dimension...  8.52 us
    reduce_scatter x1, waiting for transfers between devices, body(): lax.psum_scatter(mix_terms.astype(jnp.bfloat16), 'tp', scatter_dimension=...  8.47 us
    pallas_call x1, Pallas kernels, linear_attend(): pl.pallas_call(functools.partial(attend_kernel, head_total), out_shape=ja...  8.08 us
  transfers between devices with their start and end apart: 7, of which 7 were waited for; matrix products, arithmetic and copies ran while one was open for 4% of the time, Pallas kernels for 3%

profile of v1, /device:TPU:0, one launch (start us, length us, event | category | flops | bytes accessed | tf_op | source)
XLA Modules:
  0.0 320.1 jit_solution(8228406163420024176)
XLA Ops:
  6.5 0.0 copy-start.7
  6.5 0.0 all-gather.6.cloned.1.call-start
  6.5 2.7 convert_element_type.50
  9.3 0.0 all-gather.6.cloned.1.call-update
  9.3 0.0 reduce-scatter.3.cloned.1.call-start
  9.4 0.0 copy-done.7
  9.4 0.8 copy.17
  10.2 8.1 %shard_map.154 = bf16[256,1024]{1,0:T(8,128)(2,1)} custom-call(bf16[256,1024]{1,0:T(8,128)(2,1)} %bitcast.18, bf16[256,1024]{1,0:T(8,128)(2,1)} %bitcast.19, bf16[256,1024]{1,0:T(8,128)(2,1)} %bitcast.20, f32[256,1024]{1,0:T(8,128)} %bitcast.17, f32[256,4]{1,0:T(8,128)} %bitcast.16, f32[1,256]{1,0:T(1,128)} %bitcast.21), custom_call_target="tpu_custom_call" | custom-call | flops 1000000000 | bytes 4000000 | tf_op jit(solution)/shard_map/pallas_call | solution.py:103
  18.3 0.0 copy-start.4
  18.3 0.0 copy-start.5
  18.3 46.5 %all-gather.6.cloned.1.call-done = bf16[2048,1024]{1,0:T(8,128)(2,1)} async-done(((bf16[512,1024]{1,0:T(8,128)(2,1)}), bf16[2048,1024]{1,0:T(8,128)(2,1)}) %all-gather.6.cloned.1.call-update) | async-done | bytes 4194320 | tf_op jit(solution)/shard_map/all_gather | solution.py:150
  64.8 4.6 %convolution_convert_fusion = bf16[256,2048]{1,0:T(8,128)(2,1)} fusion(bf16[256,1024]{1,0:T(8,128)(2,1)} %shard_map.154, bf16[2048,1024]{1,0:T(8,128)(2,1)} %all-gather.6.cloned.1.call-done), kind=kOutput, calls=%fused_computation.5 | convolution fusion | flops 1074266112 | bytes 5767168 | tf_op jit(solution)/shard_map/dot_general | solution.py:121
  69.4 0.0 copy-start.1
  69.4 0.0 reduce-scatter.3.cloned.1.call-update
  69.4 0.0 all-gather.8.cloned.1.call-start
  69.5 8.5 %reduce-scatter.3.cloned.1.call-done = bf16[256,1024]{1,0:T(8,128)(2,1)} async-done(((bf16[256,2048]{1,0:T(8,128)(2,1)}), bf16[256,1024]{1,0:T(8,128)(2,1)}) %reduce-scatter.3.cloned.1.call-update) | async-done | bytes 524304 | tf_op jit(solution)/shard_map/reduce_scatter | solution.py:152
  77.9 0.0 copy-done.4
  77.9 0.0 copy-done.5
  77.9 2.0 fusion.5
  80.0 0.0 all-gather.8.cloned.1.call-update
  80.0 0.0 all-gather.10.cloned.1.call-start
  80.1 0.0 copy-done.1
  80.1 1.3 convert_element_type.57
  81.3 0.0 all-gather.10.cloned.1.call-update
  81.4 0.0 copy-start.2
  81.4 0.0 all-gather.12.cloned.1.call-start
  81.4 3.3 %convert_element_type.58 = bf16[512,1408]{1,0:T(8,128)(2,1)} convert(f32[512,1408]{1,0:T(8,128)} %param.28) | non-fusion elementwise | flops 720896 | bytes 4325376 | tf_op jit(solution)/shard_map/convert_element_type | solution.py:162
  84.7 0.0 all-gather.12.cloned.1.call-update
  84.7 0.0 all-gather.14.cloned.1.call-start
  84.7 0.0 copy-done.2
  84.8 1.3 convert_element_type.60
  86.0 0.0 copy-start.8
  86.0 0.0 copy-start.9
  86.0 0.0 all-gather.14.cloned.1.call-update
  86.1 0.0 reduce-scatter.5.cloned.1.call-start
  86.1 4.3 %all-gather.8.cloned.1.call-done = bf16[256,2048]{1,0:T(8,128)(2,1)} async-done(((bf16[256,1024]{1,0:T(8,128)(2,1)}), bf16[256,2048]{1,0:T(8,128)(2,1)}) %all-gather.8.cloned.1.call-update) | async-done | bytes 1048592 | tf_op jit(solution)/shard_map/all_gather | solution.py:157
  90.4 1.5 fusion.2
  91.9 0.0 copy-start.3
  91.9 0.0 copy-start.10
  91.9 67.0 %all-gather.10.cloned.1.call-done = bf16[2048,1408]{1,0:T(8,128)(2,1)} async-done(((bf16[512,1408]{1,0:T(8,128)(2,1)}), bf16[2048,1408]{1,0:T(8,128)(2,1)}) %all-gather.10.cloned.1.call-update) | async-done | bytes 5767184 | tf_op jit(solution)/shard_map/all_gather | solution.py:165
  159.0 0.0 copy-done.8
  159.0 0.0 copy-done.9
  159.0 4.8 %convolution_multiply_fusion.1 = f32[256,1408]{1,0:T(8,128)S(1)} fusion(bf16[2048,1408]{1,0:T(8,128)(2,1)} %all-gather.10.cloned.1.call-done, f32[1408]{0:T(1024)S(1)} %copy-done.8, bf16[256,2048]{1,0:T(8,128)(2,1)} %all-gather.8.cloned.1.call-done, f32[2048]{0:T(1024)S(1)} %copy-done.9, f32[256]{0:T(256)S(1)} %add_rsqrt_fusion), kind=kOutput, calls=%fused_computation.2 | convolution fusion | flops 1478852608 | bytes 8272384 | tf_op jit(solution)/shard_map/dot_general | solution.py:169
  163.8 0.0 copy-start
  163.8 0.0 copy-start.6
  163.8 62.5 %all-gather.12.cloned.1.call-done = bf16[2048,1408]{1,0:T(8,128)(2,1)} async-done(((bf16[512,1408]{1,0:T(8,128)(2,1)}), bf16[2048,1408]{1,0:T(8,128)(2,1)}) %all-gather.12.cloned.1.call-update) | async-done | bytes 5767184 | tf_op jit(solution)/shard_map/all_gather | solution.py:166
  226.3 67.4 %all-gather.14.cloned.1.call-done = bf16[2048,1408]{1,0:T(8,128)(2,1)} async-done(((bf16[512,1408]{1,0:T(8,128)(2,1)}), bf16[2048,1408]{1,0:T(8,128)(2,1)}) %all-gather.14.cloned.1.call-update) | async-done | bytes 5767184 | tf_op jit(solution)/shard_map/all_gather | solution.py:167
  293.7 0.0 copy-done.3
  293.7 0.0 copy-done.10
  293.7 8.9 %convolution_convert_fusion.1 = bf16[256,2048]{1,0:T(8,128)(2,1)} fusion(bf16[2048,1408]{1,0:T(8,128)(2,1)} %all-gather.14.cloned.1.call-done, bf16[2048,1408]{1,0:T(8,128)(2,1)} %all-gather.12.cloned.1.call-done, f32[256,1408]{1,0:T(8,128)S(1)} %convolution_multiply_fusion.1, f32[1408]{0:T(1024)S(1)} %copy-done.10, bf16[256,2048]{1,0:T(8,128)(2,1)S(1)} %copy-done.3, ...), kind=kOutput, calls=%fused_computation.7 | convolution fusion | flops 2957934592 | bytes 15088128 | tf_op jit(solution)/shard_map/dot_general | solution.py:121
  302.7 0.0 reduce-scatter.5.cloned.1.call-update
  302.7 8.5 %reduce-scatter.5.cloned.1.call-done = bf16[256,1024]{1,0:T(8,128)(2,1)} async-done(((bf16[256,2048]{1,0:T(8,128)(2,1)}), bf16[256,1024]{1,0:T(8,128)(2,1)}) %reduce-scatter.5.cloned.1.call-update) | async-done | bytes 524304 | tf_op jit(solution)/shard_map/reduce_scatter | solution.py:175
  311.2 0.0 copy-done
  311.2 0.0 copy-done.6
  311.2 2.0 fusion.6
  (1 shorter events, 0.0 us)
Async XLA Ops:
  6.5 2.8 copy-start.7
  6.5 58.2 %all-gather.6.cloned.1.call-start = ((), (), s32[]{:S(2)}) async-start(), calls=%async_computation.2 | async-start | bytes 5242880 | tf_op jit(solution)/shard_map/all_gather | solution.py:150
  9.3 68.6 %reduce-scatter.3.cloned.1.call-start = ((), (), s32[]{:S(2)}) async-start(), calls=%async_computation.3 | async-start | bytes 1572864 | tf_op jit(solution)/shard_map/reduce_scatter | solution.py:152
  18.3 59.7 %copy-start.4 = (bf16[1,256,1024]{2,1,0:T(8,128)(2,1)S(1)}, bf16[1,256,1024]{2,1,0:T(8,128)(2,1)}, u32[]{:S(2)}) copy-start(bf16[1,256,1024]{2,1,0:T(8,128)(2,1)} %param.16) | copy-start | bytes 1572868
  18.3 59.7 %copy-start.5 = (f32[1024]{0:T(1024)S(1)}, f32[1024]{0:T(1024)}, u32[]{:S(2)}) copy-start(f32[1024]{0:T(1024)} %param.24) | copy-start | bytes 12292
  69.4 10.7 %copy-start.1 = (f32[512,1408]{1,0:T(8,128)S(1)}, f32[512,1408]{1,0:T(8,128)}, u32[]{:S(2)}) copy-start(f32[512,1408]{1,0:T(8,128)} %param.26) | copy-start | bytes 8650756
  69.4 21.0 %all-gather.8.cloned.1.call-start = ((), (), s32[]{:S(2)}) async-start(), calls=%async_computation.4 | async-start | bytes 1572864 | tf_op jit(solution)/shard_map/all_gather | solution.py:157
  80.0 79.0 %all-gather.10.cloned.1.call-start = ((), (), s32[]{:S(2)}) async-start(), calls=%async_computation.5 | async-start | bytes 7208960 | tf_op jit(solution)/shard_map/all_gather | solution.py:165
  81.4 3.4 %copy-start.2 = (f32[512,1408]{1,0:T(8,128)S(1)}, f32[512,1408]{1,0:T(8,128)}, u32[]{:S(2)}) copy-start(f32[512,1408]{1,0:T(8,128)} %param.30) | copy-start | bytes 8650756
  81.4 145.0 %all-gather.12.cloned.1.call-start = ((), (), s32[]{:S(2)}) async-start(), calls=%async_computation.6 | async-start | bytes 7208960 | tf_op jit(solution)/shard_map/all_gather | solution.py:166
  84.7 209.0 %all-gather.14.cloned.1.call-start = ((), (), s32[]{:S(2)}) async-start(), calls=%async_computation.7 | async-start | bytes 7208960 | tf_op jit(solution)/shard_map/all_gather | solution.py:167
  86.0 72.9 %copy-start.8 = (f32[1408]{0:T(1024)S(1)}, f32[1408]{0:T(1024)}, u32[]{:S(2)}) copy-start(f32[1408]{0:T(1024)} %param.27) | copy-start | bytes 16900
  86.0 72.9 %copy-start.9 = (f32[2048]{0:T(1024)S(1)}, f32[2048]{0:T(1024)}, u32[]{:S(2)}) copy-start(f32[2048]{0:T(1024)} %param.25) | copy-start | bytes 24580
  86.1 225.2 %reduce-scatter.5.cloned.1.call-start = ((), (), s32[]{:S(2)}) async-start(), calls=%async_computation.8 | async-start | bytes 1572864 | tf_op jit(solution)/shard_map/reduce_scatter | solution.py:175
  91.9 201.8 %copy-start.3 = (bf16[256,2048]{1,0:T(8,128)(2,1)S(1)}, bf16[256,2048]{1,0:T(8,128)(2,1)}, u32[]{:S(2)}) copy-start(bf16[256,2048]{1,0:T(8,128)(2,1)} %all-gather.8.cloned.1.call-done) | copy-start | bytes 3145732
  91.9 201.8 %copy-start.10 = (f32[1408]{0:T(1024)S(1)}, f32[1408]{0:T(1024)}, u32[]{:S(2)}) copy-start(f32[1408]{0:T(1024)} %param.29) | copy-start | bytes 16900
  163.8 147.4 %copy-start = (bf16[256,1024]{1,0:T(8,128)(2,1)S(1)}, bf16[256,1024]{1,0:T(8,128)(2,1)}, u32[]{:S(2)}) copy-start(bf16[256,1024]{1,0:T(8,128)(2,1)} %fusion.5) | copy-start | bytes 1572868
  163.8 147.4 %copy-start.6 = (f32[1024]{0:T(1024)S(1)}, f32[1024]{0:T(1024)}, u32[]{:S(2)}) copy-start(f32[1024]{0:T(1024)} %param.31) | copy-start | bytes 12292
Sparse Core Ops, SparseCore 0:
  9.4 55.2 all-gather.5
  69.5 8.3 reduce-scatter.2
  80.1 10.2 all-gather.7
  92.1 66.8 all-gather.9
  160.7 65.6 all-gather.11
  228.0 65.6 all-gather.13
  302.8 8.3 reduce-scatter.4

commit v2 on v1

--- a/solution.py
+++ b/solution.py
@@ -179,9 +179,182 @@
     return result.reshape(sequence_batch, token_length, local_width)
 
 
+def exchange_kernel(axis, n, spread, count, *refs):
+    ins, outs = refs[:count], refs[count : 2 * count]
+    send_sem, recv_sem = refs[2 * count :]
+    me = lax.axis_index(axis)
+    barrier = pltpu.get_barrier_semaphore()
+    for step in range(1, n):
+        pl.semaphore_signal(
+            barrier,
+            inc=1,
+            device_id={axis: lax.rem(me + step, n)},
+            device_id_type=pl.DeviceIdType.MESH,
+        )
+    pl.semaphore_wait(barrier, n - 1)
+    copies = []
+    for step in range(1, n):
+        peer = lax.rem(me + step, n)
+        for c in range(count):
+            copy = pltpu.make_async_remote_copy(
+                src_ref=ins[c].at[peer] if spread else ins[c],
+                dst_ref=outs[c].at[me],
+                send_sem=send_sem.at[c, step - 1],
+                recv_sem=recv_sem.at[c, step - 1],
+                device_id={axis: peer},
+                device_id_type=pl.DeviceIdType.MESH,
+            )
+            copy.start()
+            copies.append(copy)
+    for c in range(count):
+        outs[c][me] = ins[c][me] if spread else ins[c][...]
+    for copy in copies:
+        copy.wait()
+
+
+def exchange(arrays, axis, n, spread, call):
+    count = len(arrays)
+    shapes = [a.shape if spread else (n,) + a.shape for a in arrays]
+    return pl.pallas_call(
+        functools.partial(exchange_kernel, axis, n, spread, count),
+        out_shape=[jax.ShapeDtypeStruct(d, a.dtype) for d, a in zip(shapes, arrays)],
+        in_specs=[pl.BlockSpec(memory_space=pltpu.VMEM)] * count,
+        out_specs=[pl.BlockSpec(memory_space=pltpu.VMEM)] * count,
+        scratch_shapes=[
+            pltpu.SemaphoreType.DMA((count, n - 1)),
+            pltpu.SemaphoreType.DMA((count, n - 1)),
+        ],
+        compiler_params=pltpu.CompilerParams(collective_id=call, has_side_effects=True),
+        cost_estimate=pl.CostEstimate(
+            flops=10**9, bytes_accessed=2 * 10**7, transcendentals=0
+        ),
+    )(*arrays)
+
+
+def moving_body(
+    sizes,
+    residual,
+    queries,
+    key_matrix,
+    value_matrix,
+    decay_logodds,
+    decay_surge,
+    head_norm_gain,
+    output_matrix,
+    output_column_scale,
+    premix_norm_gain,
+    gate_matrix,
+    gate_column_scale,
+    up_matrix,
+    up_column_scale,
+    down_matrix,
+    down_column_scale,
+):
+    n_rep, n_fs, n_tp = sizes
+    half = jnp.bfloat16
+    sequence_batch, token_length, local_width = residual.shape
+    row_count = sequence_batch * token_length
+    width = local_width * n_tp
+    own_width = output_matrix.shape[0]
+    part = own_width // n_tp
+    units = gate_matrix.shape[1] // n_fs
+    padded = -(-units // 128) * 128
+    slab = own_width // n_rep
+    rep, fs, tp = lax.axis_index("rep"), lax.axis_index("fs"), lax.axis_index("tp")
+
+    def slabs(matrix):
+        rows = lax.dynamic_slice_in_dim(matrix, rep * slab, slab, axis=0).astype(half)
+        rows = jnp.pad(rows.reshape(slab, n_fs, units), ((0, 0), (0, 0), (0, padded - units)))
+        return jnp.transpose(rows, (1, 0, 2))
+
+    weights = jnp.concatenate([slabs(m) for m in (gate_matrix, up_matrix, down_matrix)], axis=2)
+    own_rows = residual.reshape(row_count, local_width)
+    both_rows, both_scale = exchange(
+        [own_rows, output_column_scale.reshape(1, local_width)], "tp", n_tp, False, 1
+    )
+    wide = jnp.transpose(both_rows, (1, 0, 2)).reshape(row_count, n_fs, n_tp, part)
+    mine = lax.dynamic_index_in_dim(wide, tp, axis=2, keepdims=False)
+    got_weights, got_rows = exchange(
+        [weights, jnp.transpose(mine, (1, 0, 2))], "fs", n_fs, True, 2
+    )
+    all_weights = lax.all_gather(got_weights, "rep", axis=0, tiled=False)
+    all_weights = jnp.transpose(all_weights, (1, 0, 2, 3)).reshape(width, 3 * padded)
+
+    normalized_rows = linear_attend(
+        queries, key_matrix, value_matrix, decay_logodds, decay_surge, head_norm_gain
+    )
+    (gathered,) = exchange([normalized_rows], "fs", n_fs, False, 3)
+    group_rows = n_fs * row_count
+    mix_terms = by_rows(gathered.reshape(group_rows, -1), output_matrix.astype(half)).astype(half)
+    mix_split = jnp.transpose(mix_terms.reshape(group_rows, n_tp, part), (1, 0, 2))
+    (mix_parts,) = exchange([mix_split], "tp", n_tp, True, 4)
+    mixed = jnp.sum(mix_parts.astype(jnp.float32), axis=0)
+    out_scale = lax.dynamic_index_in_dim(
+        lax.dynamic_index_in_dim(both_scale.reshape(n_fs, n_tp, part), fs, 0, False), tp, 0, False
+    )
+    piece = got_rows.reshape(group_rows, part).astype(jnp.float32) + out_scale * mixed
+    (over_fs,) = exchange([piece.astype(half)], "fs", n_fs, False, 5)
+    (over_tp,) = exchange([over_fs], "tp", n_tp, False, 6)
+    updated = jnp.transpose(over_tp, (2, 1, 0, 3)).reshape(group_rows, width)
+    wide_rows = updated.astype(jnp.float32)
+    factor = lax.rsqrt(jnp.mean(wide_rows * wide_rows, axis=-1, keepdims=True) + epsilon)
+    normin = (wide_rows * factor * premix_norm_gain).astype(half)
+
+    def unit_scale(scale):
+        own = lax.dynamic_index_in_dim(scale.reshape(n_fs, units), fs, 0, False)
+        return jnp.pad(own, (0, padded - units))
+
+    both = jnp.dot(normin, all_weights[:, : 2 * padded], preferred_element_type=jnp.float32)
+    gate_pre = both[:, :padded] * unit_scale(gate_column_scale)
+    up_pre = both[:, padded:] * unit_scale(up_column_scale)
+    hidden = (jax.nn.silu(gate_pre) * up_pre).astype(half)
+    down_terms = jnp.concatenate(
+        [
+            by_rows(
+                hidden, all_weights[t * local_width : (t + 1) * local_width, 2 * padded :]
+            ).astype(half)[None]
+            for t in range(n_tp)
+        ],
+        axis=0,
+    )
+    (down_parts,) = exchange([down_terms], "tp", n_tp, True, 7)
+    down_half = jnp.sum(down_parts.astype(jnp.float32), axis=0).astype(half)
+    (down_back,) = exchange(
+        [down_half.reshape(n_fs, row_count, local_width)], "fs", n_fs, True, 8
+    )
+    down_total = jnp.sum(down_back.astype(jnp.float32), axis=0)
+    own_updated = lax.dynamic_slice(
+        updated, (fs * row_count, tp * local_width), (row_count, local_width)
+    )
+    result = (own_updated.astype(jnp.float32) + down_column_scale * down_total).astype(half)
+    return result.reshape(sequence_batch, token_length, local_width)
+
+
+def chosen_body(mesh):
+    sizes = tuple(mesh.shape[name] for name in ("rep", "fs", "tp"))
+    n_rep, n_fs, n_tp = sizes
+
+    def run(*args):
+        residual, output_matrix, gate_matrix = args[0], args[7], args[10]
+        weights = output_matrix.size + 3 * gate_matrix.size
+        rows = residual.shape[0] * residual.shape[1]
+        moved = 3 * rows * residual.shape[2] + 3 * gate_matrix.size // n_rep
+        fits = (
+            n_fs > 1
+            and n_tp > 1
+            and output_matrix.shape[0] % (128 * n_tp) == 0
+            and output_matrix.shape[0] % (16 * n_rep) == 0
+        )
+        if fits and moved < weights:
+            return moving_body(sizes, *args)
+        return body(*args)
+
+    return run
+
+
 def solution(mesh):
     return jax.shard_map(
-        body,
+        chosen_body(mesh),
         mesh=mesh,
         in_specs=(
             P(("rep", "fs"), None, "tp"),

time: 320 us -> 207 us (0.65)
  waiting for transfers between devices: 265 us -> 0.04 us
  Pallas kernels: 8.08 us -> 144 us
  local copies, waits for them, and re-layouts: 0.85 us -> 20.8 us
  matrix products: 18.4 us -> 9.93 us
  other arithmetic: 14.1 us -> 17.8 us
    all_gather x5 -> x1, waiting for transfers between devices: 248 us -> 0.02 us  [moving_body(): all_weights = lax.all_gather(got_weights, 'rep', axis=0, tiled=False)]
    pallas_call x0 -> x8, Pallas kernels: none -> 136 us  [exchange(): pl.pallas_call(functools.partial(exchange_kernel, axis, n, spread, count)...]
    reduce_scatter x2 -> x0, waiting for transfers between devices: 17 us -> none  [the longest x1 8.52 us: body(): lax.psum_scatter(down_terms.astype(jnp.bfloat16), 'tp', scatter_dimension...]
    transpose x0 -> x6, local copies, waits for them, and re-layouts: none -> 10.9 us  [the longest x1 6.31 us: moving_body(): updated = jnp.transpose(over_tp, (2, 1, 0, 3)).reshape(group_rows, width)]
    reduce_sum x1 -> x4, other arithmetic: 1.51 us -> 11.9 us  [the longest x1 5.18 us: moving_body(): down_half = jnp.sum(down_parts.astype(jnp.float32), axis=0).astype(half)]
    convert_element_type x5 -> x2, other arithmetic: 10.6 us -> 1.41 us  [the longest x1 0.95 us: moving_body(): over_fs, = exchange([piece.astype(half)], 'fs', n_fs, False, 5)]
    dot_general x2 -> x3, matrix products: 13.6 us -> 6.08 us  [by_rows(): lax.dot_general(left, right, (((1,), (1,)), ((), ())), preferred_element_...]
    dynamic_slice x0 -> x7, local copies, waits for them, and re-layouts: none -> 3.61 us  [the longest x2 1.45 us: slabs(): lax.dynamic_slice_in_dim(matrix, rep * slab, slab, axis=0).astype(half)]
  transfers between devices with their start and end apart: 7 -> 1, of which waited for: 7 -> 0; matrix products, arithmetic and copies ran while one was open for 4% -> 9% of each run, Pallas kernels for 3% -> 37%
where the time goes in v2:
time: 207 us; the launch traced here: 206 us
  Pallas kernels  144 us (70%)
  local copies, waits for them, and re-layouts  20.8 us (10%)
  other arithmetic  17.8 us (9%)
  between operations  13.7 us (7%)
  matrix products  9.93 us (5%)
    pallas_call x8, Pallas kernels, exchange(): pl.pallas_call(functools.partial(exchange_kernel, axis, n, spread, count)...  136 us
    pallas_call x1, Pallas kernels, linear_attend(): pl.pallas_call(functools.partial(attend_kernel, head_total), out_shape=ja...  8.09 us
    transpose x1, local copies, waits for them, and re-layouts, moving_body(): updated = jnp.transpose(over_tp, (2, 1, 0, 3)).reshape(group_rows, width)  6.31 us
    dot_general x3, matrix products, by_rows(): lax.dot_general(left, right, (((1,), (1,)), ((), ())), preferred_element_...  6.08 us
    reduce_sum x1, other arithmetic, moving_body(): down_half = jnp.sum(down_parts.astype(jnp.float32), axis=0).astype(half)  5.18 us
    unnamed x25, local copies, waits for them, and re-layouts  4.14 us
  transfers between devices with their start and end apart: 1, of which 0 were waited for; matrix products, arithmetic and copies ran while one was open for 9% of the time, Pallas kernels for 37%

profile of v2, /device:TPU:0, one launch (start us, length us, event | category | flops | bytes accessed | tf_op | source)
XLA Modules:
  0.0 206.4 jit_solution(2283969118512893847)
XLA Ops:
  6.5 0.0 copy-start
  6.5 0.0 all-gather.3.cloned.1.call-start
  6.5 1.8 copy-done
  8.4 0.2 copy.56
  8.6 0.2 copy.44
  8.9 1.4 constant_dynamic-slice_fusion.4
  10.3 0.2 copy.58
  10.5 0.2 copy.48
  10.8 0.2 copy.57
  11.1 0.2 copy.46
  11.3 4.1 %shard_map.154 = (bf16[2,256,1024]{2,1,0:T(8,128)(2,1)}, f32[2,1,1024]{2,1,0:T(1,128)}) custom-call(bf16[256,1024]{1,0:T(8,128)(2,1)} %bitcast.65, f32[1,1024]{1,0:T(1,128)} %bitcast.69), custom_call_target="tpu_custom_call" | custom-call | flops 1000000000 | bytes 20000000 | tf_op jit(solution)/shard_map/pallas_call | solution.py:218
  15.4 1.5 copy.49
  17.0 1.0 copy.50
  18.0 1.1 pad_maximum_fusion.1.refs_0_
  19.1 0.0 copy-start.4
  19.1 0.0 copy-start.5
  19.1 0.0 copy-start.8
  19.1 0.0 copy-start.6
  19.1 26.2 %shard_map.155 = (bf16[4,128,1152]{2,1,0:T(8,128)(2,1)}, bf16[4,256,256]{2,1,0:T(8,128)(2,1)}) custom-call(bf16[4,128,1152]{2,1,0:T(8,128)(2,1)} %pad_maximum_fusion.1.refs_0_, bf16[4,256,256]{2,1,0:T(8,128)(2,1)} %bitcast.61), custom_call_target="tpu_custom_call" | custom-call | flops 1000000000 | bytes 20000000 | tf_op jit(solution)/shard_map/pallas_call | solution.py:218
  45.3 0.0 all-gather.3.cloned.1.call-update
  45.3 0.0 copy-done.4
  45.3 0.1 reshape.77
  45.4 0.0 copy-done.5
  45.4 0.1 reshape.78
  45.5 0.0 copy-done.8
  45.5 0.8 copy.51
  46.3 0.0 copy-done.6
  46.4 8.1 %shard_map.156.refs_0_ = bf16[256,1024]{1,0:T(8,128)(2,1)} custom-call(bf16[256,1024]{1,0:T(8,128)(2,1)} %bitcast.66, bf16[256,1024]{1,0:T(8,128)(2,1)} %bitcast.67, bf16[256,1024]{1,0:T(8,128)(2,1)} %bitcast.68, f32[256,1024]{1,0:T(8,128)} %bitcast.64, f32[256,4]{1,0:T(8,128)} %bitcast.62, f32[1,256]{1,0:T(1,128)} %bitcast.70), custom_call_target="tpu_custom_call" | custom-call | flops 1000000000 | bytes 4000000 | tf_op jit(solution)/shard_map/pallas_call | solution.py:103
  54.5 28.5 %shard_map.157 = bf16[4,256,1024]{2,1,0:T(8,128)(2,1)} custom-call(bf16[256,1024]{1,0:T(8,128)(2,1)} %shard_map.156.refs_0_), custom_call_target="tpu_custom_call" | custom-call | flops 1000000000 | bytes 20000000 | tf_op jit(solution)/shard_map/pallas_call | solution.py:218
  83.0 3.5 %convolution_convert_fusion = bf16[1024,512]{0,1:T(8,128)(2,1)S(1)} fusion(bf16[1024,1024]{1,0:T(8,128)(2,1)} %bitcast.71, f32[512,1024]{1,0:T(8,128)} %param.23), kind=kOutput, calls=%fused_computation.15 | convolution fusion | flops 1074790400 | bytes 5242880 | tf_op jit(solution)/shard_map/dot_general | solution.py:121
  86.5 1.3 copy.52
  87.9 0.0 copy-start.3
  87.9 4.2 %shard_map.158 = bf16[2,1024,256]{2,1,0:T(8,128)(2,1)} custom-call(bf16[2,1024,256]{2,1,0:T(8,128)(2,1)} %bitcast.60), custom_call_target="tpu_custom_call" | custom-call | flops 1000000000 | bytes 20000000 | tf_op jit(solution)/shard_map/pallas_call | solution.py:218
  92.1 1.5 convert_reduce_fusion.1
  93.6 0.0 copy-done.3
  93.6 1.0 fusion.6.refs_0_
  94.6 27.8 %shard_map.159.refs_0_ = bf16[4,1024,256]{2,1,0:T(8,128)(2,1)} custom-call(bf16[1024,256]{1,0:T(8,128)(2,1)} %fusion.6.refs_0_), custom_call_target="tpu_custom_call" | custom-call | flops 1000000000 | bytes 20000000 | tf_op jit(solution)/shard_map/pallas_call | solution.py:218
  122.4 7.8 %shard_map.160 = bf16[2,4,1024,256]{3,2,1,0:T(8,128)(2,1)} custom-call(bf16[4,1024,256]{2,1,0:T(8,128)(2,1)} %shard_map.159.refs_0_), custom_call_target="tpu_custom_call" | custom-call | flops 1000000000 | bytes 20000000 | tf_op jit(solution)/shard_map/pallas_call | solution.py:218
  130.2 6.3 %copy.53 = bf16[1024,4,2,256]{0,3,2,1:T(8,128)(2,1)} copy(bf16[1024,4,2,256]{3,0,1,2:T(8,128)(2,1)} %bitcast.46) | data formatting | bytes 8388608 | tf_op jit(solution)/shard_map/transpose | solution.py:298
  136.5 1.1 dynamic_slice.34
  137.6 0.2 copy.59
  137.8 3.1 %multiply_reduce_fusion = f32[1024]{0:T(1024)S(1)} fusion(bf16[2,4,1024,256]{3,2,1,0:T(8,128)(2,1)} %shard_map.160), kind=kLoop, calls=%fused_computation.1 | loop fusion | flops 6290432 | bytes 4198400 | tf_op jit(solution)/shard_map/reduce_sum | solution.py:300
  140.9 0.0 all-gather.3.cloned.1.call-done
  140.9 0.0 copy-start.2
  140.9 0.0 copy-start.9
  140.9 3.0 %copy.55 = bf16[4,4,128,1152]{3,2,1,0:T(8,128)(2,1)S(1)} copy(bf16[4,4,128,1152]{3,2,0,1:T(8,128)(2,1)} %bitcast.50) | data formatting | bytes 9437184 | tf_op jit(solution)/shard_map/transpose | solution.py:281
  143.9 0.6 copy-done.2
  144.5 0.0 copy-done.9
  144.5 3.9 %fusion = f32[1024,768]{1,0:T(8,128)S(1)} fusion(bf16[1024,2048]{0,1:T(8,128)(2,1)S(1)} %bitcast.49, f32[2048]{0:T(1024)S(1)} %copy-done.9, f32[1024]{0:T(1024)S(1)} %add_rsqrt_fusion, bf16[2048,1152]{1,0:T(8,128)(2,1)S(1)} %bitcast.51), kind=kOutput, calls=%fused_computation.2 | convolution fusion | flops 3229614080 | bytes 10498048 | tf_op jit(solution)/shard_map/dot_general | solution.py:307
  148.4 0.5 fusion.5
  148.8 1.3 convert_bitcast_fusion
  150.1 1.3 convert_bitcast_fusion.1
  151.4 2.3 %pad_maximum_fusion.refs_0_ = bf16[2,1024,1024]{2,1,0:T(8,128)(2,1)} fusion(bf16[1,1024,1024]{2,1,0:T(8,128)(2,1)S(1)} %convert_bitcast_fusion, bf16[1,1024,1024]{2,1,0:T(8,128)(2,1)S(1)} %convert_bitcast_fusion.1), kind=kLoop, calls=%fused_computation.3 | loop fusion | flops 2097152 | bytes 8388608 | tf_op jit(solution)/shard_map/concatenate | solution.py:311
  153.7 8.3 %shard_map.161 = bf16[2,1024,1024]{2,1,0:T(8,128)(2,1)} custom-call(bf16[2,1024,1024]{2,1,0:T(8,128)(2,1)} %pad_maximum_fusion.refs_0_), custom_call_target="tpu_custom_call" | custom-call | flops 1000000000 | bytes 20000000 | tf_op jit(solution)/shard_map/pallas_call | solution.py:218
  162.0 5.2 %reduce_sum.41 = bf16[1024,1024]{1,0:T(8,128)(2,1)} reduce(bf16[2,1024,1024]{2,1,0:T(8,128)(2,1)} %shard_map.161, bf16[]{:T(256)} %constant.62.clone.1), dimensions={0}, to_apply=%region_2.3 | reduce | flops 1048576 | bytes 6291458 | tf_op jit(solution)/shard_map/reduce_sum | solution.py:321
  167.2 0.0 copy-start.1
  167.2 29.2 %shard_map.162 = bf16[4,256,1024]{2,1,0:T(8,128)(2,1)} custom-call(bf16[4,256,1024]{2,1,0:T(8,128)(2,1)} %bitcast.47), custom_call_target="tpu_custom_call" | custom-call | flops 1000000000 | bytes 20000000 | tf_op jit(solution)/shard_map/pallas_call | solution.py:218
  196.5 0.0 copy-start.7
  196.5 2.1 %convert_reduce_fusion = f32[256,1024]{1,0:T(8,128)S(1)} fusion(bf16[4,256,1024]{2,1,0:T(8,128)(2,1)} %shard_map.162), kind=kLoop, calls=%fused_computation.4 | loop fusion | flops 1835008 | bytes 3145728 | tf_op jit(solution)/shard_map/reduce_sum | solution.py:325
  198.6 0.0 copy-done.7
  198.6 1.0 fusion.10
  199.6 0.0 copy-done.1
  (12 shorter events, 0.3 us)
Async XLA Ops:
  6.5 1.8 copy-start
  6.5 134.3 %all-gather.3.cloned.1.call-start = ((), (), s32[]{:S(2)}) async-start(), calls=%async_computation | async-start | bytes 5898240 | tf_op jit(solution)/shard_map/all_gather | solution.py:280
  19.1 26.2 %copy-start.4 = (f32[1408]{0:T(1024)S(1)}, f32[1408]{0:T(1024)}, u32[]{:S(2)}) copy-start(f32[1408]{0:T(1024)} %param.27) | copy-start | bytes 16900
  19.1 26.3 %copy-start.5 = (f32[1408]{0:T(1024)S(1)}, f32[1408]{0:T(1024)}, u32[]{:S(2)}) copy-start(f32[1408]{0:T(1024)} %param.29) | copy-start | bytes 16900
  19.1 26.4 %copy-start.8 = (f32[1,256,4]{1,2,0:T(4,128)S(1)}, f32[1,256,4]{1,2,0:T(4,128)}, u32[]{:S(2)}) copy-start(f32[1,256,4]{1,2,0:T(4,128)} %param.21) | copy-start | bytes 12292
  19.1 27.2 %copy-start.6 = (f32[2,1,1024]{2,1,0:T(1,128)S(1)}, f32[2,1,1024]{2,1,0:T(1,128)}, u32[]{:S(2)}) copy-start(f32[2,1,1024]{2,1,0:T(1,128)} %get-tuple-element.11) | copy-start | bytes 24580
  87.9 5.8 %copy-start.3 = (bf16[4,256,256]{2,1,0:T(8,128)(2,1)S(1)}, bf16[4,256,256]{2,1,0:T(8,128)(2,1)}, u32[]{:S(2)}) copy-start(bf16[4,256,256]{2,1,0:T(8,128)(2,1)} %get-tuple-element.10) | copy-start | bytes 1572868
  140.9 3.6 %copy-start.2 = (bf16[1024,4,2,256]{0,3,2,1:T(8,128)(2,1)S(1)}, bf16[1024,4,2,256]{0,3,2,1:T(8,128)(2,1)}, u32[]{:S(2)}) copy-start(bf16[1024,4,2,256]{0,3,2,1:T(8,128)(2,1)} %copy.53) | copy-start | bytes 12582916
  140.9 3.6 %copy-start.9 = (f32[2048]{0:T(1024)S(1)}, f32[2048]{0:T(1024)}, u32[]{:S(2)}) copy-start(f32[2048]{0:T(1024)} %param.25) | copy-start | bytes 24580
  167.2 32.4 %copy-start.1 = (f32[512,1408]{1,0:T(8,128)S(1)}, f32[512,1408]{1,0:T(8,128)}, u32[]{:S(2)}) copy-start(f32[512,1408]{1,0:T(8,128)} %param.26) | copy-start | bytes 8650756
  196.5 2.1 %copy-start.7 = (f32[1024]{0:T(1024)S(1)}, f32[1024]{0:T(1024)}, u32[]{:S(2)}) copy-start(f32[1024]{0:T(1024)} %param.31) | copy-start | bytes 12292
Sparse Core Ops, SparseCore 0:
  45.4 90.4 all-gather.2

commit v3 on v2

--- a/solution.py
+++ b/solution.py
@@ -229,6 +229,129 @@
             flops=10**9, bytes_accessed=2 * 10**7, transcendentals=0
         ),
     )(*arrays)
+
+
+def send(source, target, sems, index, device):
+    copy = pltpu.make_async_remote_copy(
+        src_ref=source,
+        dst_ref=target,
+        send_sem=sems[0].at[index],
+        recv_sem=sems[1].at[index],
+        device_id=device,
+        device_id_type=pl.DeviceIdType.MESH,
+    )
+    copy.start()
+    return copy
+
+
+def greet(devices):
+    barrier = pltpu.get_barrier_semaphore()
+    for device in devices:
+        pl.semaphore_signal(
+            barrier, inc=1, device_id=device, device_id_type=pl.DeviceIdType.MESH
+        )
+    pl.semaphore_wait(barrier, len(devices))
+
+
+def gather_kernel(share, x_ref, out_ref, *sems):
+    me, tp = lax.axis_index("fs"), lax.axis_index("tp")
+    near = me + 1 - 2 * lax.rem(me, 2)
+    far = lax.rem(me + 2, 4)
+    corner = lax.rem(near + 2, 4)
+    to_near, to_far, to_pair = {"fs": near}, {"fs": far}, {"tp": 1 - tp}
+    greet([to_near, to_far] + ([to_pair] if share else []))
+    own = out_ref.at[tp] if share else out_ref
+    rows = x_ref.shape[0] // 2
+    upper, lower = pl.ds(0, rows), pl.ds(rows, rows)
+    near_upper = send(x_ref.at[upper], own.at[me, upper], sems, 0, to_near)
+    far_lower = send(x_ref.at[lower], own.at[me, lower], sems, 1, to_far)
+    near_lower = send(x_ref.at[lower], own.at[me, lower], sems, 2, to_near)
+    far_upper = send(x_ref.at[upper], own.at[me, upper], sems, 3, to_far)
+    copies = [near_upper, far_lower, near_lower, far_upper]
+    shared = [send(x_ref, own.at[me], sems, 6, to_pair)] if share else []
+    own[me] = x_ref[...]
+    near_upper.wait_recv()
+    corner_upper = send(own.at[near, upper], own.at[near, upper], sems, 4, to_far)
+    far_lower.wait_recv()
+    corner_lower = send(own.at[far, lower], own.at[far, lower], sems, 5, to_near)
+    near_lower.wait_recv()
+    if share:
+        shared.append(send(own.at[near], own.at[near], sems, 7, to_pair))
+    far_upper.wait_recv()
+    if share:
+        shared.append(send(own.at[far], own.at[far], sems, 8, to_pair))
+    corner_upper.wait_recv()
+    corner_lower.wait_recv()
+    if share:
+        shared.append(send(own.at[corner], own.at[corner], sems, 9, to_pair))
+    for copy in copies + [corner_upper, corner_lower]:
+        copy.wait_send()
+    for copy in shared:
+        copy.wait()
+
+
+def gather(x, n_fs, n_tp, share, call):
+    shape = ((n_tp,) if share else ()) + (n_fs,) + x.shape
+    return pl.pallas_call(
+        functools.partial(gather_kernel, share),
+        out_shape=jax.ShapeDtypeStruct(shape, x.dtype),
+        in_specs=[pl.BlockSpec(memory_space=pltpu.VMEM)],
+        out_specs=pl.BlockSpec(memory_space=pltpu.VMEM),
+        scratch_shapes=[pltpu.SemaphoreType.DMA((10,)), pltpu.SemaphoreType.DMA((10,))],
+        compiler_params=pltpu.CompilerParams(collective_id=call, has_side_effects=True),
+        cost_estimate=pl.CostEstimate(
+            flops=10**9, bytes_accessed=2 * 10**7, transcendentals=0
+        ),
+    )(x)
+
+
+def reduce_kernel(n, terms_ref, back_ref, part_ref, total_ref, *sems):
+    me, tp = lax.axis_index("fs"), lax.axis_index("tp")
+    steps = list(range(1, n)) + [0]
+    peers = [lax.rem(me + step, n) for step in range(n)]
+    greet([{"fs": peers[step]} for step in range(1, n)] + [{"tp": 1 - tp}])
+    pairs = {
+        step: send(
+            terms_ref.at[1 - tp, peers[step]], part_ref.at[peers[step]], sems, step, {"tp": 1 - tp}
+        )
+        for step in steps
+    }
+    copies = []
+    for step in steps:
+        peer = peers[step]
+        pairs[step].wait_recv()
+        total = terms_ref[tp, peer].astype(jnp.float32) + part_ref[peer].astype(jnp.float32)
+        if step == 0:
+            back_ref[me] = total.astype(back_ref.dtype)
+        else:
+            total_ref[peer] = total.astype(back_ref.dtype)
+            copies.append(
+                send(total_ref.at[peer], back_ref.at[me], sems, n + step, {"fs": peer})
+            )
+    for step in steps:
+        pairs[step].wait_send()
+    for copy in copies:
+        copy.wait()
+
+
+def reduce_back(terms, n_fs, call):
+    shape = terms.shape[1:]
+    return pl.pallas_call(
+        functools.partial(reduce_kernel, n_fs),
+        out_shape=jax.ShapeDtypeStruct(shape, terms.dtype),
+        in_specs=[pl.BlockSpec(memory_space=pltpu.VMEM)],
+        out_specs=pl.BlockSpec(memory_space=pltpu.VMEM),
+        scratch_shapes=[
+            pltpu.VMEM(shape, terms.dtype),
+            pltpu.VMEM(shape, terms.dtype),
+            pltpu.SemaphoreType.DMA((2 * n_fs,)),
+            pltpu.SemaphoreType.DMA((2 * n_fs,)),
+        ],
+        compiler_params=pltpu.CompilerParams(collective_id=call, has_side_effects=True),
+        cost_estimate=pl.CostEstimate(
+            flops=10**9, bytes_accessed=2 * 10**7, transcendentals=0
+        ),
+    )(terms)
 
 
 def moving_body(
@@ -283,7 +406,7 @@
     normalized_rows = linear_attend(
         queries, key_matrix, value_matrix, decay_logodds, decay_surge, head_norm_gain
     )
-    (gathered,) = exchange([normalized_rows], "fs", n_fs, False, 3)
+    gathered = gather(normalized_rows, n_fs, n_tp, False, 3)
     group_rows = n_fs * row_count
     mix_terms = by_rows(gathered.reshape(group_rows, -1), output_matrix.astype(half)).astype(half)
     mix_split = jnp.transpose(mix_terms.reshape(group_rows, n_tp, part), (1, 0, 2))
@@ -293,9 +416,8 @@
         lax.dynamic_index_in_dim(both_scale.reshape(n_fs, n_tp, part), fs, 0, False), tp, 0, False
     )
     piece = got_rows.reshape(group_rows, part).astype(jnp.float32) + out_scale * mixed
-    (over_fs,) = exchange([piece.astype(half)], "fs", n_fs, False, 5)
-    (over_tp,) = exchange([over_fs], "tp", n_tp, False, 6)
-    updated = jnp.transpose(over_tp, (2, 1, 0, 3)).reshape(group_rows, width)
+    everywhere = gather(piece.astype(half), n_fs, n_tp, True, 5)
+    updated = jnp.transpose(everywhere, (2, 1, 0, 3)).reshape(group_rows, width)
     wide_rows = updated.astype(jnp.float32)
     factor = lax.rsqrt(jnp.mean(wide_rows * wide_rows, axis=-1, keepdims=True) + epsilon)
     normin = (wide_rows * factor * premix_norm_gain).astype(half)
@@ -317,10 +439,8 @@
         ],
         axis=0,
     )
-    (down_parts,) = exchange([down_terms], "tp", n_tp, True, 7)
-    down_half = jnp.sum(down_parts.astype(jnp.float32), axis=0).astype(half)
-    (down_back,) = exchange(
-        [down_half.reshape(n_fs, row_count, local_width)], "fs", n_fs, True, 8
+    down_back = reduce_back(
+        down_terms.reshape(n_tp, n_fs, row_count, local_width), n_fs, 7
     )
     down_total = jnp.sum(down_back.astype(jnp.float32), axis=0)
     own_updated = lax.dynamic_slice(
@@ -340,8 +460,8 @@
         rows = residual.shape[0] * residual.shape[1]
         moved = 3 * rows * residual.shape[2] + 3 * gate_matrix.size // n_rep
         fits = (
-            n_fs > 1
-            and n_tp > 1
+            n_fs == 4
+            and n_tp == 2
             and output_matrix.shape[0] % (128 * n_tp) == 0
             and output_matrix.shape[0] % (16 * n_rep) == 0
         )

time: 207 us -> 204 us (0.986)
  Pallas kernels: 144 us -> 121 us
  local copies, waits for them, and re-layouts: 20.8 us -> 33.4 us
  waiting for transfers between devices: 0.04 us -> 9.95 us
  other arithmetic: 17.8 us -> 13.8 us
    pallas_call x8 -> x3, Pallas kernels: 136 us -> 34.4 us  [exchange(): pl.pallas_call(functools.partial(exchange_kernel, axis, n, spread, count)...]
    pallas_call x0 -> x3, Pallas kernels: none -> 78.5 us  [the longest x2 46.6 us: gather(): pl.pallas_call(functools.partial(gather_kernel, share), out_shape=jax.Sha...]
    all_gather x1, waiting for transfers between devices: 0.02 us -> 9.94 us  [moving_body(): all_weights = lax.all_gather(got_weights, 'rep', axis=0, tiled=False)]
    reduce_sum x1 -> x0, other arithmetic: 5.18 us -> none  [moving_body(): down_half = jnp.sum(down_parts.astype(jnp.float32), axis=0).astype(half)]
    unnamed x25, local copies, waits for them, and re-layouts: 4.14 us -> 8 us
    reshape x3, local copies, waits for them, and re-layouts: 0.66 us -> 3.58 us  [slabs(): rows.reshape(slab, n_fs, units)]
    transpose x3, local copies, waits for them, and re-layouts: 0.14 us -> 2.4 us  [slabs(): return jnp.transpose(rows, (1, 0, 2))]
  transfers between devices with their start and end apart: 1 -> 1, of which waited for: 0 -> 1; matrix products, arithmetic and copies ran while one was open for 9% -> 11% of each run, Pallas kernels for 37% -> 29%
where the time goes in v3:
time: 204 us; the launch traced here: 203 us
  Pallas kernels  121 us (59%)
  local copies, waits for them, and re-layouts  33.4 us (16%)
  other arithmetic  13.8 us (7%)
  between operations  13.6 us (7%)
  matrix products  10.9 us (5%)
  waiting for transfers between devices  9.95 us (5%)
    pallas_call x2, Pallas kernels, gather(): pl.pallas_call(functools.partial(gather_kernel, share), out_shape=jax.Sha...  46.6 us
    pallas_call x3, Pallas kernels, exchange(): pl.pallas_call(functools.partial(exchange_kernel, axis, n, spread, count)...  34.4 us
    pallas_call x1, Pallas kernels, reduce_back(): pl.pallas_call(functools.partial(reduce_kernel, n_fs), out_shape=jax.Shap...  31.9 us
    all_gather x1, waiting for transfers between devices, moving_body(): all_weights = lax.all_gather(got_weights, 'rep', axis=0, tiled=False)  9.94 us
    pallas_call x1, Pallas kernels, linear_attend(): pl.pallas_call(functools.partial(attend_kernel, head_total), out_shape=ja...  8.09 us
    unnamed x25, local copies, waits for them, and re-layouts  8 us
    dot_general x3, matrix products, by_rows(): lax.dot_general(left, right, (((1,), (1,)), ((), ())), preferred_element_...  7.05 us
    transpose x1, local copies, waits for them, and re-layouts, moving_body(): updated = jnp.transpose(everywhere, (2, 1, 0, 3)).reshape(group_rows, width)  6.31 us
  transfers between devices with their start and end apart: 1, of which 1 were waited for; matrix products, arithmetic and copies ran while one was open for 11% of the time, Pallas kernels for 29%

profile of v3, /device:TPU:0, one launch (start us, length us, event | category | flops | bytes accessed | tf_op | source)
XLA Modules:
  0.0 202.7 jit_solution(10955910851061255874)
XLA Ops:
  6.5 0.0 copy-start
  6.5 0.0 all-gather.3.cloned.1.call-start
  6.5 1.8 copy-done
  8.4 0.9 copy.56
  9.3 1.2 copy.44
  10.5 0.8 pad_bitcast_fusion.2
  11.3 2.1 %constant_dynamic-slice_fusion.4 = (bf16[128,1408]{1,0:T(8,128)(2,1)S(1)}, bf16[128,1408]{1,0:T(8,128)(2,1)}) fusion(f32[512,1408]{1,0:T(8,128)} %param.30, s32[]{:T(128)S(6)} %select_n.28, f32[512,1408]{1,0:T(8,128)} %param.28), kind=kLoop, calls=%fused_computation.32 | loop fusion | bytes 1441796 | tf_op jit(solution)/shard_map/dynamic_slice | solution.py:389
  13.5 0.9 copy.58
  14.4 1.2 copy.48
  15.6 0.8 pad_bitcast_fusion
  16.4 1.9 copy.57
  18.2 1.2 copy.46
  19.4 0.8 pad_bitcast_fusion.1
  20.2 4.1 %shard_map.154 = (bf16[2,256,1024]{2,1,0:T(8,128)(2,1)}, f32[2,1,1024]{2,1,0:T(1,128)}) custom-call(bf16[256,1024]{1,0:T(8,128)(2,1)} %bitcast.63, f32[1,1024]{1,0:T(1,128)} %bitcast.67), custom_call_target="tpu_custom_call" | custom-call | flops 1000000000 | bytes 20000000 | tf_op jit(solution)/shard_map/pallas_call | solution.py:218
  24.4 2.3 %copy.49 = bf16[256,2,1024]{0,2,1:T(8,128)(2,1)} copy(bf16[256,2,1024]{2,0,1:T(8,128)(2,1)} %bitcast.56) | data formatting | bytes 2097152 | tf_op jit(solution)/shard_map/transpose | solution.py:398
  26.6 1.1 constant_dynamic-slice_fusion.3
  27.7 1.0 copy.50
  28.7 2.3 %pad_maximum_fusion.1.refs_0_ = bf16[4,128,1152]{2,1,0:T(8,128)(2,1)} fusion(bf16[4,128,384]{2,1,0:T(8,128)(2,1)} %pad_bitcast_fusion, bf16[4,128,384]{2,1,0:T(8,128)(2,1)} %pad_bitcast_fusion.1, bf16[4,128,384]{2,1,0:T(8,128)(2,1)} %pad_bitcast_fusion.2), kind=kLoop, calls=%fused_computation.16 | loop fusion | flops 3538944 | bytes 2359296 | tf_op jit(solution)/shard_map/concatenate | solution.py:393
  31.1 0.0 copy-start.4
  31.1 0.0 copy-start.5
  31.1 0.0 copy-start.8
  31.1 0.0 copy-start.6
  31.1 26.1 %shard_map.155 = (bf16[4,128,1152]{2,1,0:T(8,128)(2,1)}, bf16[4,256,256]{2,1,0:T(8,128)(2,1)}) custom-call(bf16[4,128,1152]{2,1,0:T(8,128)(2,1)} %pad_maximum_fusion.1.refs_0_, bf16[4,256,256]{2,1,0:T(8,128)(2,1)} %bitcast.59), custom_call_target="tpu_custom_call" | custom-call | flops 1000000000 | bytes 20000000 | tf_op jit(solution)/shard_map/pallas_call | solution.py:218
  57.2 0.0 all-gather.3.cloned.1.call-update
  57.3 0.0 copy-done.4
  57.3 0.1 reshape.79
  57.4 0.0 copy-done.5
  57.4 0.1 reshape.80
  57.5 0.0 copy-done.8
  57.5 0.8 copy.51
  58.3 0.0 copy-done.6
  58.4 8.1 %shard_map.156.x_ref = bf16[256,1024]{1,0:T(8,128)(2,1)} custom-call(bf16[256,1024]{1,0:T(8,128)(2,1)} %bitcast.64, bf16[256,1024]{1,0:T(8,128)(2,1)} %bitcast.65, bf16[256,1024]{1,0:T(8,128)(2,1)} %bitcast.66, f32[256,1024]{1,0:T(8,128)} %bitcast.62, f32[256,4]{1,0:T(8,128)} %bitcast.60, f32[1,256]{1,0:T(1,128)} %bitcast.68), custom_call_target="tpu_custom_call" | custom-call | flops 1000000000 | bytes 4000000 | tf_op jit(solution)/shard_map/pallas_call | solution.py:103
  66.4 22.2 %shard_map.157 = bf16[4,256,1024]{2,1,0:T(8,128)(2,1)} custom-call(bf16[256,1024]{1,0:T(8,128)(2,1)} %shard_map.156.x_ref), custom_call_target="tpu_custom_call" | custom-call | flops 1000000000 | bytes 20000000 | tf_op jit(solution)/shard_map/pallas_call | solution.py:295
  88.7 4.5 %convolution_convert_fusion.2 = bf16[1024,512]{0,1:T(8,128)(2,1)} fusion(bf16[1024,1024]{1,0:T(8,128)(2,1)} %bitcast.69, f32[512,1024]{1,0:T(8,128)} %param.23), kind=kOutput, calls=%fused_computation.15 | convolution fusion | flops 1074790400 | bytes 5242880 | tf_op jit(solution)/shard_map/dot_general | solution.py:121
  93.2 2.3 %copy.52 = bf16[1024,2,256]{2,0,1:T(8,128)(2,1)} copy(bf16[1024,2,256]{0,2,1:T(8,128)(2,1)} %bitcast.57) | data formatting | bytes 2097152 | tf_op jit(solution)/shard_map/reshape | solution.py:412
  95.4 0.0 copy-start.3
  95.4 4.2 %shard_map.158 = bf16[2,1024,256]{2,1,0:T(8,128)(2,1)} custom-call(bf16[2,1024,256]{2,1,0:T(8,128)(2,1)} %bitcast.58), custom_call_target="tpu_custom_call" | custom-call | flops 1000000000 | bytes 20000000 | tf_op jit(solution)/shard_map/pallas_call | solution.py:218
  99.7 1.5 convert_reduce_fusion.1
  101.2 0.0 copy-done.3
  101.2 1.0 fusion.6.x_ref
  102.1 24.3 %shard_map.159 = bf16[2,4,1024,256]{3,2,1,0:T(8,128)(2,1)} custom-call(bf16[1024,256]{1,0:T(8,128)(2,1)} %fusion.6.x_ref), custom_call_target="tpu_custom_call" | custom-call | flops 1000000000 | bytes 20000000 | tf_op jit(solution)/shard_map/pallas_call | solution.py:295
  126.5 6.3 %copy.53 = bf16[1024,4,2,256]{0,3,2,1:T(8,128)(2,1)} copy(bf16[1024,4,2,256]{3,0,1,2:T(8,128)(2,1)} %bitcast.43) | data formatting | bytes 8388608 | tf_op jit(solution)/shard_map/transpose | solution.py:420
  132.8 1.1 dynamic_slice.34
  133.9 1.0 copy.59
  134.9 3.1 %multiply_reduce_fusion = f32[1024]{0:T(1024)S(1)} fusion(bf16[2,4,1024,256]{3,2,1,0:T(8,128)(2,1)} %shard_map.159), kind=kLoop, calls=%fused_computation.1 | loop fusion | flops 6290432 | bytes 4198400 | tf_op jit(solution)/shard_map/reduce_sum | solution.py:422
  138.0 9.9 %all-gather.3.cloned.1.call-done = bf16[16,128,1152]{2,1,0:T(8,128)(2,1)} async-done(((bf16[4,128,1152]{2,1,0:T(8,128)(2,1)}), bf16[16,128,1152]{2,1,0:T(8,128)(2,1)}) %all-gather.3.cloned.1.call-update) | async-done | bytes 4718608 | tf_op jit(solution)/shard_map/all_gather | solution.py:403
  147.9 0.0 copy-start.1
  147.9 0.0 copy-start.9
  147.9 2.9 %copy.55 = bf16[4,4,128,1152]{3,2,1,0:T(8,128)(2,1)S(1)} copy(bf16[4,4,128,1152]{3,2,0,1:T(8,128)(2,1)} %bitcast.46) | data formatting | bytes 9437184 | tf_op jit(solution)/shard_map/transpose | solution.py:404
  150.9 0.6 copy-done.1
  151.5 0.0 copy-done.9
  151.5 3.9 %fusion = f32[1024,768]{1,0:T(8,128)S(1)} fusion(bf16[1024,2048]{0,1:T(8,128)(2,1)S(1)} %bitcast.45, f32[2048]{0:T(1024)S(1)} %copy-done.9, f32[1024]{0:T(1024)S(1)} %add_rsqrt_fusion, bf16[2048,1152]{1,0:T(8,128)(2,1)S(1)} %bitcast.47), kind=kOutput, calls=%fused_computation.2 | convolution fusion | flops 3229614080 | bytes 10498048 | tf_op jit(solution)/shard_map/dot_general | solution.py:429
  155.4 0.5 fusion.5
  155.9 1.3 convolution_convert_fusion
  157.1 1.3 convolution_convert_fusion.1
  158.4 2.3 %pad_maximum_fusion.terms_ref = bf16[2,4,256,1024]{3,2,1,0:T(8,128)(2,1)} fusion(bf16[1,4,256,1024]{3,2,1,0:T(8,128)(2,1)S(1)} %bitcast.51, bf16[1,4,256,1024]{3,2,1,0:T(8,128)(2,1)S(1)} %bitcast.52), kind=kLoop, calls=%fused_computation.3 | loop fusion | flops 2097152 | bytes 8388608 | tf_op jit(solution)/shard_map/concatenate | solution.py:433
  160.7 31.9 %shard_map.160 = bf16[4,256,1024]{2,1,0:T(8,128)(2,1)} custom-call(bf16[2,4,256,1024]{3,2,1,0:T(8,128)(2,1)} %pad_maximum_fusion.terms_ref), custom_call_target="tpu_custom_call" | custom-call | flops 1000000000 | bytes 20000000 | tf_op jit(solution)/shard_map/pallas_call | solution.py:339
  192.7 0.0 copy-start.2
  192.7 0.0 copy-start.7
  192.7 2.2 %convert_reduce_fusion = f32[256,1024]{1,0:T(8,128)S(1)} fusion(bf16[4,256,1024]{2,1,0:T(8,128)(2,1)} %shard_map.160), kind=kLoop, calls=%fused_computation.4 | loop fusion | flops 1835008 | bytes 3145728 | tf_op jit(solution)/shard_map/reduce_sum | solution.py:445
  194.8 0.0 copy-done.2
  194.8 0.0 copy-done.7
  194.9 1.0 fusion.10
  (8 shorter events, 0.1 us)
Async XLA Ops:
  6.5 1.8 copy-start
  6.5 141.4 %all-gather.3.cloned.1.call-start = ((), (), s32[]{:S(2)}) async-start(), calls=%async_computation | async-start | bytes 5898240 | tf_op jit(solution)/shard_map/all_gather | solution.py:403
  31.1 26.2 %copy-start.4 = (f32[1408]{0:T(1024)S(1)}, f32[1408]{0:T(1024)}, u32[]{:S(2)}) copy-start(f32[1408]{0:T(1024)} %param.27) | copy-start | bytes 16900
  31.1 26.3 %copy-start.5 = (f32[1408]{0:T(1024)S(1)}, f32[1408]{0:T(1024)}, u32[]{:S(2)}) copy-start(f32[1408]{0:T(1024)} %param.29) | copy-start | bytes 16900
  31.1 26.4 %copy-start.8 = (f32[1,256,4]{1,2,0:T(4,128)S(1)}, f32[1,256,4]{1,2,0:T(4,128)}, u32[]{:S(2)}) copy-start(f32[1,256,4]{1,2,0:T(4,128)} %param.21) | copy-start | bytes 12292
  31.1 27.2 %copy-start.6 = (f32[2,1,1024]{2,1,0:T(1,128)S(1)}, f32[2,1,1024]{2,1,0:T(1,128)}, u32[]{:S(2)}) copy-start(f32[2,1,1024]{2,1,0:T(1,128)} %get-tuple-element.11) | copy-start | bytes 24580
  95.4 5.7 %copy-start.3 = (bf16[4,256,256]{2,1,0:T(8,128)(2,1)S(1)}, bf16[4,256,256]{2,1,0:T(8,128)(2,1)}, u32[]{:S(2)}) copy-start(bf16[4,256,256]{2,1,0:T(8,128)(2,1)} %get-tuple-element.10) | copy-start | bytes 1572868
  147.9 3.6 %copy-start.1 = (bf16[1024,4,2,256]{0,3,2,1:T(8,128)(2,1)S(1)}, bf16[1024,4,2,256]{0,3,2,1:T(8,128)(2,1)}, u32[]{:S(2)}) copy-start(bf16[1024,4,2,256]{0,3,2,1:T(8,128)(2,1)} %copy.53) | copy-start | bytes 12582916
  147.9 3.6 %copy-start.9 = (f32[2048]{0:T(1024)S(1)}, f32[2048]{0:T(1024)}, u32[]{:S(2)}) copy-start(f32[2048]{0:T(1024)} %param.25) | copy-start | bytes 24580
  192.7 2.2 %copy-start.2 = (bf16[256,1024]{1,0:T(8,128)(2,1)S(1)}, bf16[256,1024]{1,0:T(8,128)(2,1)}, u32[]{:S(2)}) copy-start(bf16[256,1024]{1,0:T(8,128)(2,1)} %copy.59) | copy-start | bytes 1572868
  192.7 2.2 %copy-start.7 = (f32[1024]{0:T(1024)S(1)}, f32[1024]{0:T(1024)}, u32[]{:S(2)}) copy-start(f32[1024]{0:T(1024)} %param.31) | copy-start | bytes 12292
Sparse Core Ops, SparseCore 0:
  57.4 90.4 all-gather.2

commit v4 on v3

--- a/solution.py
+++ b/solution.py
@@ -354,6 +354,42 @@
     )(terms)
 
 
+def pack_kernel(n, units, padded, *refs):
+    matrices, out_ref, held, sems = refs[:3], refs[3], refs[4], refs[5]
+    slab = held.shape[1]
+    rows = pl.ds(pl.multiple_of(lax.axis_index("rep") * slab, slab), slab)
+    copies = [
+        pltpu.make_async_copy(matrix.at[rows], held.at[m], sems.at[m])
+        for m, matrix in enumerate(matrices)
+    ]
+    for copy in copies:
+        copy.start()
+    for m, copy in enumerate(copies):
+        copy.wait()
+        for j in range(n):
+            own = held[m, :, j * units : (j + 1) * units]
+            if padded > units:
+                fill = jnp.zeros((slab, padded - units), own.dtype)
+                own = jnp.concatenate([own, fill], axis=1)
+            out_ref[j, :, m * padded : (m + 1) * padded] = own.astype(out_ref.dtype)
+
+
+def pack(matrices, n, units, padded, slab):
+    return pl.pallas_call(
+        functools.partial(pack_kernel, n, units, padded),
+        out_shape=jax.ShapeDtypeStruct((n, slab, 3 * padded), jnp.bfloat16),
+        in_specs=[pl.BlockSpec(memory_space=pl.ANY)] * 3,
+        out_specs=pl.BlockSpec(memory_space=pltpu.VMEM),
+        scratch_shapes=[
+            pltpu.VMEM((3, slab, matrices[0].shape[1]), jnp.float32),
+            pltpu.SemaphoreType.DMA((3,)),
+        ],
+        cost_estimate=pl.CostEstimate(
+            flops=10**6, bytes_accessed=4 * 10**6, transcendentals=0
+        ),
+    )(*matrices)
+
+
 def moving_body(
     sizes,
     residual,
@@ -385,12 +421,7 @@
     slab = own_width // n_rep
     rep, fs, tp = lax.axis_index("rep"), lax.axis_index("fs"), lax.axis_index("tp")
 
-    def slabs(matrix):
-        rows = lax.dynamic_slice_in_dim(matrix, rep * slab, slab, axis=0).astype(half)
-        rows = jnp.pad(rows.reshape(slab, n_fs, units), ((0, 0), (0, 0), (0, padded - units)))
-        return jnp.transpose(rows, (1, 0, 2))
-
-    weights = jnp.concatenate([slabs(m) for m in (gate_matrix, up_matrix, down_matrix)], axis=2)
+    weights = pack((gate_matrix, up_matrix, down_matrix), n_fs, units, padded, slab)
     own_rows = residual.reshape(row_count, local_width)
     both_rows, both_scale = exchange(
         [own_rows, output_column_scale.reshape(1, local_width)], "tp", n_tp, False, 1

time: 204 us -> 188 us (0.922)
  local copies, waits for them, and re-layouts: 33.4 us -> 16.1 us
  waiting for transfers between devices: 9.95 us -> 13.1 us
  Pallas kernels: 121 us -> 124 us
  other arithmetic: 13.8 us -> 11.4 us
    unnamed x25 -> x20, local copies, waits for them, and re-layouts: 8 us -> 1.7 us
    reshape x3 -> x0, local copies, waits for them, and re-layouts: 3.58 us -> none  [slabs(): rows.reshape(slab, n_fs, units)]
    all_gather x1, waiting for transfers between devices: 9.94 us -> 13.1 us  [moving_body(): all_weights = lax.all_gather(got_weights, 'rep', axis=0, tiled=False)]
    pallas_call x0 -> x1, Pallas kernels: none -> 2.74 us  [pack(): pl.pallas_call(functools.partial(pack_kernel, n, units, padded), out_shap...]
    transpose x3 -> x0, local copies, waits for them, and re-layouts: 2.4 us -> none  [slabs(): return jnp.transpose(rows, (1, 0, 2))]
    concatenate x1 -> x0, other arithmetic: 2.35 us -> none  [moving_body(): jnp.concatenate([slabs(m) for m in (gate_matrix, up_matrix, down_matrix)]...]
    dynamic_slice x2 -> x0, local copies, waits for them, and re-layouts: 2.18 us -> none  [slabs(): lax.dynamic_slice_in_dim(matrix, rep * slab, slab, axis=0).astype(half)]
  transfers between devices with their start and end apart: 1 -> 1, of which waited for: 1 -> 1; matrix products, arithmetic and copies ran while one was open for 11% -> 10% of each run, Pallas kernels for 29% -> 31%
where the time goes in v4:
time: 188 us; the launch traced here: 187 us
  Pallas kernels  124 us (66%)
  local copies, waits for them, and re-layouts  16.1 us (9%)
  between operations  13.7 us (7%)
  waiting for transfers between devices  13.1 us (7%)
  other arithmetic  11.4 us (6%)
  matrix products  9.3 us (5%)
    pallas_call x2, Pallas kernels, gather(): pl.pallas_call(functools.partial(gather_kernel, share), out_shape=jax.Sha...  46.6 us
    pallas_call x3, Pallas kernels, exchange(): pl.pallas_call(functools.partial(exchange_kernel, axis, n, spread, count)...  34.4 us
    pallas_call x1, Pallas kernels, reduce_back(): pl.pallas_call(functools.partial(reduce_kernel, n_fs), out_shape=jax.Shap...  31.9 us
    all_gather x1, waiting for transfers between devices, moving_body(): all_weights = lax.all_gather(got_weights, 'rep', axis=0, tiled=False)  13.1 us
    pallas_call x1, Pallas kernels, linear_attend(): pl.pallas_call(functools.partial(attend_kernel, head_total), out_shape=ja...  8.24 us
    transpose x1, local copies, waits for them, and re-layouts, moving_body(): updated = jnp.transpose(everywhere, (2, 1, 0, 3)).reshape(group_rows, width)  6.31 us
    dot_general x3, matrix products, by_rows(): lax.dot_general(left, right, (((1,), (1,)), ((), ())), preferred_element_...  5.44 us
    dot_general x1, matrix products, moving_body(): jnp.dot(normin, all_weights[:, :2 * padded], preferred_element_type=jnp.f...  3.86 us
  transfers between devices with their start and end apart: 1, of which 1 were waited for; matrix products, arithmetic and copies ran while one was open for 10% of the time, Pallas kernels for 31%

profile of v4, /device:TPU:0, one launch (start us, length us, event | category | flops | bytes accessed | tf_op | source)
XLA Modules:
  0.0 187.5 jit_solution(3790522598793054070)
XLA Ops:
  6.5 0.0 all-gather.3.cloned.1.call-start
  6.5 4.1 %shard_map.155 = (bf16[2,256,1024]{2,1,0:T(8,128)(2,1)}, f32[2,1,1024]{2,1,0:T(1,128)}) custom-call(bf16[256,1024]{1,0:T(8,128)(2,1)} %bitcast.51, f32[1,1024]{1,0:T(1,128)} %bitcast.55), custom_call_target="tpu_custom_call" | custom-call | flops 1000000000 | bytes 20000000 | tf_op jit(solution)/shard_map/pallas_call | solution.py:218
  10.7 1.5 copy.31
  12.2 1.0 copy.32
  13.2 2.7 %shard_map.154.refs_0_ = bf16[4,128,1152]{2,1,0:T(8,128)(2,1)} custom-call(f32[512,1408]{1,0:T(8,128)} %refs_0_.1, f32[512,1408]{1,0:T(8,128)} %refs_1_.1, f32[512,1408]{1,0:T(8,128)} %refs_2_.1), custom_call_target="tpu_custom_call" | custom-call | flops 1000000 | bytes 4000000 | tf_op jit(solution)/shard_map/pallas_call | solution.py:378
  15.9 0.0 copy-start.2
  15.9 0.0 copy-start.3
  16.0 0.0 copy-start.6
  16.0 0.0 copy-start.4
  16.0 26.1 %shard_map.156 = (bf16[4,128,1152]{2,1,0:T(8,128)(2,1)}, bf16[4,256,256]{2,1,0:T(8,128)(2,1)}) custom-call(bf16[4,128,1152]{2,1,0:T(8,128)(2,1)} %shard_map.154.refs_0_, bf16[4,256,256]{2,1,0:T(8,128)(2,1)} %bitcast.47), custom_call_target="tpu_custom_call" | custom-call | flops 1000000000 | bytes 20000000 | tf_op jit(solution)/shard_map/pallas_call | solution.py:218
  42.1 0.0 all-gather.3.cloned.1.call-update
  42.1 0.0 copy-done.2
  42.2 0.1 reshape.67
  42.2 0.0 copy-done.3
  42.2 0.1 reshape.68
  42.4 0.0 copy-done.6
  42.4 0.8 copy.33
  43.2 0.0 copy-done.4
  43.2 0.0 copy-start.7
  43.3 8.2 %shard_map.157.x_ref = bf16[256,1024]{1,0:T(8,128)(2,1)} custom-call(bf16[256,1024]{1,0:T(8,128)(2,1)} %bitcast.52, bf16[256,1024]{1,0:T(8,128)(2,1)} %bitcast.53, bf16[256,1024]{1,0:T(8,128)(2,1)} %bitcast.54, f32[256,1024]{1,0:T(8,128)} %bitcast.50, f32[256,4]{1,0:T(8,128)} %bitcast.48, f32[1,256]{1,0:T(1,128)} %bitcast.56), custom_call_target="tpu_custom_call" | custom-call | flops 1000000000 | bytes 4000000 | tf_op jit(solution)/shard_map/pallas_call | solution.py:103
  51.5 22.2 %shard_map.158 = bf16[4,256,1024]{2,1,0:T(8,128)(2,1)} custom-call(bf16[256,1024]{1,0:T(8,128)(2,1)} %shard_map.157.x_ref), custom_call_target="tpu_custom_call" | custom-call | flops 1000000000 | bytes 20000000 | tf_op jit(solution)/shard_map/pallas_call | solution.py:295
  73.7 0.0 copy-done.7
  73.7 2.9 %convolution_convert_fusion.2 = bf16[1024,512]{0,1:T(8,128)(2,1)S(1)} fusion(bf16[1024,1024]{1,0:T(8,128)(2,1)} %bitcast.57, f32[512,1024]{1,0:T(8,128)S(1)} %copy-done.7), kind=kOutput, calls=%fused_computation.15 | convolution fusion | flops 1074790400 | bytes 5242880 | tf_op jit(solution)/shard_map/dot_general | solution.py:121
  76.6 1.3 copy.34
  77.9 0.0 copy-start.1
  78.0 4.2 %shard_map.159 = bf16[2,1024,256]{2,1,0:T(8,128)(2,1)} custom-call(bf16[2,1024,256]{2,1,0:T(8,128)(2,1)} %bitcast.46), custom_call_target="tpu_custom_call" | custom-call | flops 1000000000 | bytes 20000000 | tf_op jit(solution)/shard_map/pallas_call | solution.py:218
  82.2 1.5 convert_reduce_fusion.1
  83.7 0.0 copy-done.1
  83.7 1.0 fusion.6.x_ref
  84.7 24.3 %shard_map.160 = bf16[2,4,1024,256]{3,2,1,0:T(8,128)(2,1)} custom-call(bf16[1024,256]{1,0:T(8,128)(2,1)} %fusion.6.x_ref), custom_call_target="tpu_custom_call" | custom-call | flops 1000000000 | bytes 20000000 | tf_op jit(solution)/shard_map/pallas_call | solution.py:295
  109.0 6.3 %copy.35 = bf16[1024,4,2,256]{0,3,2,1:T(8,128)(2,1)} copy(bf16[1024,4,2,256]{3,0,1,2:T(8,128)(2,1)} %bitcast.34) | data formatting | bytes 8388608 | tf_op jit(solution)/shard_map/transpose | solution.py:451
  115.4 1.1 dynamic_slice.22
  116.4 0.2 copy.38
  116.7 3.1 %multiply_reduce_fusion = f32[1024]{0:T(1024)S(1)} fusion(bf16[2,4,1024,256]{3,2,1,0:T(8,128)(2,1)} %shard_map.160), kind=kLoop, calls=%fused_computation.1 | loop fusion | flops 6290432 | bytes 4198400 | tf_op jit(solution)/shard_map/reduce_sum | solution.py:453
  119.7 13.1 %all-gather.3.cloned.1.call-done = bf16[16,128,1152]{2,1,0:T(8,128)(2,1)} async-done(((bf16[4,128,1152]{2,1,0:T(8,128)(2,1)}), bf16[16,128,1152]{2,1,0:T(8,128)(2,1)}) %all-gather.3.cloned.1.call-update) | async-done | bytes 4718608 | tf_op jit(solution)/shard_map/all_gather | solution.py:434
  132.8 0.0 copy-start
  132.8 0.0 copy-start.8
  132.8 2.9 %copy.37 = bf16[4,4,128,1152]{3,2,1,0:T(8,128)(2,1)S(1)} copy(bf16[4,4,128,1152]{3,2,0,1:T(8,128)(2,1)} %bitcast.37) | data formatting | bytes 9437184 | tf_op jit(solution)/shard_map/transpose | solution.py:435
  135.8 0.6 copy-done
  136.4 0.0 copy-done.8
  136.4 3.9 %fusion = f32[1024,768]{1,0:T(8,128)S(1)} fusion(bf16[1024,2048]{0,1:T(8,128)(2,1)S(1)} %bitcast.36, f32[2048]{0:T(1024)S(1)} %copy-done.8, f32[1024]{0:T(1024)S(1)} %add_rsqrt_fusion, bf16[2048,1152]{1,0:T(8,128)(2,1)S(1)} %bitcast.38), kind=kOutput, calls=%fused_computation.2 | convolution fusion | flops 3229614080 | bytes 10498048 | tf_op jit(solution)/shard_map/dot_general | solution.py:460
  140.3 0.5 fusion.5
  140.7 1.3 convolution_convert_fusion
  142.0 1.3 convolution_convert_fusion.1
  143.3 2.3 %pad_maximum_fusion.terms_ref = bf16[2,4,256,1024]{3,2,1,0:T(8,128)(2,1)} fusion(bf16[1,4,256,1024]{3,2,1,0:T(8,128)(2,1)S(1)} %bitcast.42, bf16[1,4,256,1024]{3,2,1,0:T(8,128)(2,1)S(1)} %bitcast.43), kind=kLoop, calls=%fused_computation.3 | loop fusion | flops 2097152 | bytes 8388608 | tf_op jit(solution)/shard_map/concatenate | solution.py:464
  145.6 31.9 %shard_map.161 = bf16[4,256,1024]{2,1,0:T(8,128)(2,1)} custom-call(bf16[2,4,256,1024]{3,2,1,0:T(8,128)(2,1)} %pad_maximum_fusion.terms_ref), custom_call_target="tpu_custom_call" | custom-call | flops 1000000000 | bytes 20000000 | tf_op jit(solution)/shard_map/pallas_call | solution.py:339
  177.5 0.0 copy-start.5
  177.5 2.1 %convert_reduce_fusion = f32[256,1024]{1,0:T(8,128)S(1)} fusion(bf16[4,256,1024]{2,1,0:T(8,128)(2,1)} %shard_map.161), kind=kLoop, calls=%fused_computation.4 | loop fusion | flops 1835008 | bytes 3145728 | tf_op jit(solution)/shard_map/reduce_sum | solution.py:476
  179.7 0.0 copy-done.5
  179.7 1.0 fusion.10
  (8 shorter events, 0.1 us)
Async XLA Ops:
  6.5 126.3 %all-gather.3.cloned.1.call-start = ((), (), s32[]{:S(2)}) async-start(), calls=%async_computation | async-start | bytes 5898240 | tf_op jit(solution)/shard_map/all_gather | solution.py:434
  15.9 26.2 %copy-start.2 = (f32[1408]{0:T(1024)S(1)}, f32[1408]{0:T(1024)}, u32[]{:S(2)}) copy-start(f32[1408]{0:T(1024)} %param.27) | copy-start | bytes 16900
  15.9 26.3 %copy-start.3 = (f32[1408]{0:T(1024)S(1)}, f32[1408]{0:T(1024)}, u32[]{:S(2)}) copy-start(f32[1408]{0:T(1024)} %param.29) | copy-start | bytes 16900
  16.0 26.4 %copy-start.6 = (f32[1,256,4]{1,2,0:T(4,128)S(1)}, f32[1,256,4]{1,2,0:T(4,128)}, u32[]{:S(2)}) copy-start(f32[1,256,4]{1,2,0:T(4,128)} %param.21) | copy-start | bytes 12292
  16.0 27.2 %copy-start.4 = (f32[2,1,1024]{2,1,0:T(1,128)S(1)}, f32[2,1,1024]{2,1,0:T(1,128)}, u32[]{:S(2)}) copy-start(f32[2,1,1024]{2,1,0:T(1,128)} %get-tuple-element.11) | copy-start | bytes 24580
  43.2 30.5 %copy-start.7 = (f32[512,1024]{1,0:T(8,128)S(1)}, f32[512,1024]{1,0:T(8,128)}, u32[]{:S(2)}) copy-start(f32[512,1024]{1,0:T(8,128)} %param.23) | copy-start | bytes 6291460
  77.9 5.8 %copy-start.1 = (bf16[4,256,256]{2,1,0:T(8,128)(2,1)S(1)}, bf16[4,256,256]{2,1,0:T(8,128)(2,1)}, u32[]{:S(2)}) copy-start(bf16[4,256,256]{2,1,0:T(8,128)(2,1)} %get-tuple-element.10) | copy-start | bytes 1572868
  132.8 3.6 %copy-start = (bf16[1024,4,2,256]{0,3,2,1:T(8,128)(2,1)S(1)}, bf16[1024,4,2,256]{0,3,2,1:T(8,128)(2,1)}, u32[]{:S(2)}) copy-start(bf16[1024,4,2,256]{0,3,2,1:T(8,128)(2,1)} %copy.35) | copy-start | bytes 12582916
  132.8 3.6 %copy-start.8 = (f32[2048]{0:T(1024)S(1)}, f32[2048]{0:T(1024)}, u32[]{:S(2)}) copy-start(f32[2048]{0:T(1024)} %param.25) | copy-start | bytes 24580
  177.5 2.1 %copy-start.5 = (f32[1024]{0:T(1024)S(1)}, f32[1024]{0:T(1024)}, u32[]{:S(2)}) copy-start(f32[1024]{0:T(1024)} %param.31) | copy-start | bytes 12292
Sparse Core Ops, SparseCore 0:
  42.3 90.4 all-gather.2
